TPU v7x, 256 devices: a whole 4x4x8 slice. The times are simulated.
256 devices in a mesh: sp: 32 (over z, y), tp: 8 (over x, core).
Axes of the slice: x: 4, y: 4, z: 8, core: 2. Of those that a mesh axis runs over, the one named last changes fastest.
Arguments:
- tokens: bfloat16 [32768, 2048], P('sp'), may hold values from -6 to 6
- in_gain: float32 [2048], replicated, may hold values from 0.1 to 1.9
- w_query: bfloat16 [2048, 1024], P(None, 'tp'), may hold values from -0.125 to 0.125
- w_forget: bfloat16 [2048, 1024], P(None, 'tp'), may hold values from -0.125 to 0.125
- w_input: bfloat16 [2048, 1024], P(None, 'tp'), may hold values from -0.125 to 0.125
- w_outgate: bfloat16 [2048, 1024], P(None, 'tp'), may hold values from -0.125 to 0.125
- w_conv_h: bfloat16 [2048, 1024], P(None, 'tp'), may hold values from -0.125 to 0.125
- w_conv_b: bfloat16 [2048, 1024], P(None, 'tp'), may hold values from -0.125 to 0.125
- w_conv_c: bfloat16 [2048, 1024], P(None, 'tp'), may hold values from -0.125 to 0.125
- forget_floor: float32 [1024], P('tp'), may hold values from 0.84 to 1
- forget_leak: float32 [32768, 1024], P('sp', 'tp'), may hold values from -1 to 0
- state_gain: float32 [128], replicated, may hold values from 0.1 to 1.9
- conv_taps: bfloat16 [3, 1024], P(None, 'tp'), may hold values from -3.5 to 3.5
- group_gain: float32 [128], replicated, may hold values from 0.1 to 1.9
- out_state: bfloat16 [1024, 2048], P('tp'), may hold values from -0.1875 to 0.1875
- out_conv: bfloat16 [1024, 2048], P('tp'), may hold values from -0.1875 to 0.1875
Outputs:
- mixed_out: bfloat16 [32768, 2048], P('sp', 'tp')
All inputs are finite; a program needn't handle non-finite values.
Results may differ from a plain program's by a relative error of at most 0.015.
Values may be sent and summed in bfloat16 or wider, within the bound.
No kernel may reach another device: no remote copies, remote signals or barrier semaphores. Data moves between devices by JAX's collectives and lax.ppermute only.
A program may use at most 128 MiB of HBM per device.

v0:
```python
import jax
import jax.numpy as jnp
from jax import lax
from jax.experimental import pallas as pl
from jax.experimental.pallas import tpu as pltpu
from jax.sharding import Mesh
from jax.sharding import PartitionSpec as P


F = 128
BLOCK = 64
TAPS = 3
STEP = 256
FRONT = 256
PACK = F + 16
EPS = 1e-06
f32 = jnp.float32
bf16 = jnp.bfloat16


def dot(a, b, dims=((1,), (0,))):
    return lax.dot_general(a, b, (dims, ((), ())), preferred_element_type=f32)


def rms(values, gain):
    return values * lax.rsqrt(jnp.mean(values * values, axis=-1, keepdims=True) + EPS) * gain


def silu(x):
    return x * jax.nn.sigmoid(x)


def put_message(ref, state, decay):
    high = decay.astype(bf16)
    low = (decay - high.astype(f32)).astype(bf16)
    ref[:F] = state.astype(bf16)
    row = lax.broadcasted_iota(jnp.int32, (16, F), 0)
    ref[F:] = jnp.where(row == 0, high.astype(f32), jnp.where(row == 1, low.astype(f32), 0.0)).astype(bf16)


def get_message(ref):
    tail = ref[F:].astype(f32)
    return ref[:F].astype(f32), tail[0:1] + tail[1:2]


def front_kernel(tokens, gain, w_forget, w_input, floor, leak,
                 normed, keys, values, cums, message,
                 weights, gates):
    step = pl.program_id(0)

    @pl.when(step == 0)
    def _():
        weights[:, :F] = w_forget[...]
        weights[:, F:] = w_input[...]

    n = rms(tokens[...].astype(f32), gain[...]).astype(bf16)
    normed[...] = n
    rows = pl.ds(pl.multiple_of(step * FRONT, FRONT), FRONT)
    gates[rows] = dot(n, weights[...]).astype(bf16)

    @pl.when(step == pl.num_programs(0) - 1)
    def _():
        row = lax.broadcasted_iota(jnp.int32, (STEP, STEP), 0)
        col = lax.broadcasted_iota(jnp.int32, (STEP, STEP), 1)
        tri = jnp.where(row >= col, 1.0, 0.0).astype(bf16)
        state = jnp.zeros((F, F), f32)
        total = jnp.zeros((1, F), f32)
        for at in range(0, gates.shape[0], STEP):
            value = gates[at : at + STEP, F:]
            values[at : at + STEP] = value
            gate = gates[at : at + STEP, :F].astype(f32)
            key = (1.0 - floor[...]) * jax.nn.sigmoid(-gate)
            keys[at : at + STEP] = key
            log_forget = jnp.log1p(-key) + leak[at : at + STEP]
            high = log_forget.astype(bf16)
            rest = log_forget - high.astype(f32)
            mid = rest.astype(bf16)
            low = (rest - mid.astype(f32)).astype(bf16)
            cum = dot(tri, high) + dot(tri, mid) + dot(tri, low)
            cums[at : at + STEP] = cum
            last = cum[STEP - 1 : STEP]
            fresh = dot(value, (key * jnp.exp(last - cum)).astype(bf16), ((0,), (0,)))
            state = state * jnp.exp(last) + fresh
            total = total + last
        put_message(message, state, jnp.exp(total))


def grant(mib, **more):
    return pltpu.CompilerParams(vmem_limit_bytes=mib * 2**20, **more)


def front(tokens, gain, w_forget, w_input, floor, leak):
    count, width = tokens.shape
    whole = lambda s: (0, 0)
    line = lambda s: (s, 0)
    return pl.pallas_call(
        front_kernel,
        grid=(count // FRONT,),
        in_specs=[
            pl.BlockSpec((FRONT, width), line),
            pl.BlockSpec((1, width), whole),
            pl.BlockSpec((width, F), whole),
            pl.BlockSpec((width, F), whole),
            pl.BlockSpec((1, F), whole),
            pl.BlockSpec((count, F), whole),
        ],
        out_specs=[
            pl.BlockSpec((FRONT, width), line),
            pl.BlockSpec((count, F), whole),
            pl.BlockSpec((count, F), whole),
            pl.BlockSpec((count, F), whole),
            pl.BlockSpec((PACK, F), whole),
        ],
        out_shape=[
            jax.ShapeDtypeStruct((count, width), bf16),
            jax.ShapeDtypeStruct((count, F), f32),
            jax.ShapeDtypeStruct((count, F), bf16),
            jax.ShapeDtypeStruct((count, F), f32),
            jax.ShapeDtypeStruct((PACK, F), bf16),
        ],
        scratch_shapes=[
            pltpu.VMEM((width, 2 * F), bf16),
            pltpu.VMEM((count, 2 * F), bf16),
        ],
        compiler_params=grant(60, dimension_semantics=("arbitrary",)),
        name="front",
    )(tokens, gain, w_forget, w_input, floor, leak)


def read_kernel(normed, w_query, w_outgate, gain, keys, values, cums,
                reads, carries, gates, weights, state, total):
    @pl.when(pl.program_id(0) == 0)
    def _():
        weights[:, :F] = w_query[...]
        weights[:, F:] = w_outgate[...]
        state[...] = jnp.zeros_like(state)
        total[...] = jnp.zeros_like(total)

    both = dot(normed[...], weights[...]).astype(bf16).astype(f32)
    query = silu(both[:, :F])
    gates[...] = silu(both[:, F:]) * gain[...]
    row = lax.broadcasted_iota(jnp.int32, (BLOCK, BLOCK), 0)
    col = lax.broadcasted_iota(jnp.int32, (BLOCK, BLOCK), 1)
    start = state[...]
    before = total[0:1]
    base = jnp.zeros((1, F), f32)
    for b in range(STEP // BLOCK):
        at = b * BLOCK
        q = query[at : at + BLOCK]
        k = keys[at : at + BLOCK]
        v = values[at : at + BLOCK]
        edge = cums[at + BLOCK - 1 : at + BLOCK]
        c = cums[at : at + BLOCK] - base
        half = c[BLOCK // 2 - 1 : BLOCK // 2]
        last = edge - base
        scores = dot((q * jnp.exp(c - half)).astype(bf16), (k * jnp.exp(half - c)).astype(bf16), ((1,), (1,)))
        scores = jnp.where(row >= col, scores, 0.0).astype(bf16)
        faded = q * jnp.exp(c)
        reads[at : at + BLOCK] = dot(scores, v) + dot(faded.astype(bf16), start.astype(bf16), ((1,), (1,)))
        carries[at : at + BLOCK] = (faded * jnp.exp(before + base)).astype(bf16)
        fresh = dot(v, (k * jnp.exp(last - c)).astype(bf16), ((0,), (0,)))
        start = start * jnp.exp(last) + fresh
        base = edge
    state[...] = start
    total[...] = jnp.broadcast_to(before + base, total.shape)


def read(normed, w_query, w_outgate, gain, keys, values, cums):
    count, width = normed.shape
    whole = lambda s: (0, 0)
    line = lambda s: (s, 0)
    return pl.pallas_call(
        read_kernel,
        grid=(count // STEP,),
        in_specs=[
            pl.BlockSpec((STEP, width), line),
            pl.BlockSpec((width, F), whole),
            pl.BlockSpec((width, F), whole),
            pl.BlockSpec((1, F), whole),
            pl.BlockSpec((STEP, F), line),
            pl.BlockSpec((STEP, F), line),
            pl.BlockSpec((STEP, F), line),
        ],
        out_specs=[pl.BlockSpec((STEP, F), line)] * 3,
        out_shape=[
            jax.ShapeDtypeStruct((count, F), f32),
            jax.ShapeDtypeStruct((count, F), bf16),
            jax.ShapeDtypeStruct((count, F), f32),
        ],
        scratch_shapes=[
            pltpu.VMEM((width, 2 * F), bf16),
            pltpu.VMEM((F, F), f32),
            pltpu.VMEM((8, F), f32),
        ],
        compiler_params=grant(16, dimension_semantics=("arbitrary",)),
        name="read",
    )(normed, w_query, w_outgate, gain, keys, values, cums)


def conv_kernel(first, normed, rim, in_gain, w_h, w_c, w_b, taps, gain, result, weights, window):
    step = pl.program_id(0)

    @pl.when(step == 0)
    def _():
        weights[:, :F] = w_h[...]
        weights[:, F:] = w_c[...]
        edge = rms(rim[...].astype(f32), in_gain[...]).astype(bf16)
        both = dot(edge, weights[...]).astype(bf16).astype(f32)
        signal = (both[:, :F] * both[:, F:]).astype(bf16).astype(f32)
        window[:8] = jnp.where(first[0] > 0, 0.0, signal[8:])

    @pl.when(step > 0)
    def _():
        window[:8] = window[STEP:]

    both = dot(normed[...], weights[...]).astype(bf16).astype(f32)
    window[8:] = (both[:, :F] * both[:, F:]).astype(bf16).astype(f32)
    scale = taps[...].astype(f32)
    total = scale[0:1] * window[6 : 6 + STEP]
    total = total + scale[1:2] * window[7 : 7 + STEP]
    total = total + scale[2:3] * window[8 : 8 + STEP]
    after = dot(normed[...], w_b[...]).astype(bf16).astype(f32)
    result[...] = rms(after * total, gain[...]).astype(bf16)


def conv(first, normed, rim, in_gain, w_h, w_c, w_b, taps, gain):
    count, width = normed.shape
    whole = lambda s: (0, 0)
    line = lambda s: (s, 0)
    return pl.pallas_call(
        conv_kernel,
        grid=(count // STEP,),
        in_specs=[
            pl.BlockSpec(memory_space=pltpu.SMEM),
            pl.BlockSpec((STEP, width), line),
            pl.BlockSpec((16, width), whole),
            pl.BlockSpec((1, width), whole),
            pl.BlockSpec((width, F), whole),
            pl.BlockSpec((width, F), whole),
            pl.BlockSpec((width, F), whole),
            pl.BlockSpec((TAPS, F), whole),
            pl.BlockSpec((1, F), whole),
        ],
        out_specs=pl.BlockSpec((STEP, F), line),
        out_shape=jax.ShapeDtypeStruct((count, F), bf16),
        scratch_shapes=[pltpu.VMEM((width, 2 * F), bf16), pltpu.VMEM((STEP + 8, F), f32)],
        compiler_params=grant(16, dimension_semantics=("arbitrary",)),
        name="conv",
    )(first, normed, rim, in_gain, w_h, w_c, w_b, taps, gain)


def row_kernel(index, own, one, two, three, total, before, fade):
    y = index[0]
    parts = [get_message(r) for r in (own, one, two, three)]
    place = [jnp.where(y >= d, y - d, y - d + 4) for d in range(4)]
    whole, inside = 0.0, 0.0
    product, product_before = 1.0, 1.0
    for d, (state, decay) in enumerate(parts):
        later = jnp.ones_like(decay)
        between = jnp.ones_like(decay)
        for other, (_, factor) in enumerate(parts):
            if other == d:
                continue
            behind = place[other] > place[d]
            later = later * jnp.where(behind, factor, 1.0)
            between = between * jnp.where(behind & (place[other] < y), factor, 1.0)
        whole = whole + state * later
        inside = inside + state * jnp.where(place[d] < y, between, 0.0)
        product = product * decay
        product_before = product_before * jnp.where(place[d] < y, decay, 1.0)
    put_message(total, whole, product)
    before[...] = inside
    fade[...] = jnp.broadcast_to(product_before, fade.shape)


def column_kernel(index, own, one, two, three, window, before, fade):
    z = index[0]
    state, product = jnp.zeros((F, F), f32), jnp.ones((1, F), f32)
    for d, ref in ((3, three), (2, two), (1, one)):
        piece, decay = get_message(ref)
        decay = jnp.where(z >= d, decay, 1.0)
        state = state * decay + jnp.where(z >= d, piece, 0.0)
        product = product * decay
    piece, decay = get_message(own)
    put_message(window, state * decay + piece, product * decay)
    before[...] = state
    fade[...] = jnp.broadcast_to(product, fade.shape)


def join(kernel, index, *messages):
    vmem = pl.BlockSpec(memory_space=pltpu.VMEM)
    return pl.pallas_call(
        kernel,
        in_specs=[pl.BlockSpec(memory_space=pltpu.SMEM)] + [vmem] * 4,
        out_specs=[vmem] * 3,
        out_shape=[
            jax.ShapeDtypeStruct((PACK, F), bf16),
            jax.ShapeDtypeStruct((F, F), f32),
            jax.ShapeDtypeStruct((8, F), f32),
        ],
        compiler_params=grant(4),
    )(index, *messages)


def finish_kernel(index, far, column, column_fade, row, row_fade, carries, reads, gates, result):
    piece, _ = get_message(far)
    piece = jnp.where(index[0] >= 4, piece, 0.0)
    incoming = (column[...] + piece * column_fade[0:1]) * row_fade[0:1] + row[...]
    found = reads[...] + dot(carries[...], incoming.astype(bf16), ((1,), (1,)))
    result[...] = rms(found, gates[...]).astype(bf16)


def finish(index, far, column, column_fade, row, row_fade, carries, reads, gates):
    vmem = pl.BlockSpec(memory_space=pltpu.VMEM)
    return pl.pallas_call(
        finish_kernel,
        in_specs=[pl.BlockSpec(memory_space=pltpu.SMEM)] + [vmem] * 8,
        out_specs=vmem,
        out_shape=jax.ShapeDtypeStruct(reads.shape, bf16),
        compiler_params=grant(12),
        name="finish",
    )(index, far, column, column_fade, row, row_fade, carries, reads, gates)


def half_kernel(*refs):
    parts, weights, out = refs[:4], refs[4:8], refs[8]
    out[...] = dot(
        jnp.concatenate([r[...] for r in parts], axis=1),
        jnp.concatenate([r[F:] for r in weights], axis=0),
    )


def last_kernel(*refs):
    parts, weights, earlier, kept, sent = refs[:4], refs[4:8], refs[8], refs[9], refs[10]
    total = earlier[...] + dot(
        jnp.concatenate([r[...] for r in parts], axis=1),
        jnp.concatenate([r[:F] for r in weights], axis=0),
    )
    width = total.shape[1] // 2
    kept[...] = total[:, :width]
    sent[...] = total[:, width:].astype(bf16)


def project_half(parts, weights):
    vmem = pl.BlockSpec(memory_space=pltpu.VMEM)
    return pl.pallas_call(
        half_kernel,
        in_specs=[vmem] * 8,
        out_specs=vmem,
        out_shape=jax.ShapeDtypeStruct((parts[0].shape[0], weights[0].shape[1]), f32),
        compiler_params=grant(16),
        name="half",
    )(*parts, *weights)


def project_last(parts, weights, earlier):
    vmem = pl.BlockSpec(memory_space=pltpu.VMEM)
    count, width = earlier.shape
    return pl.pallas_call(
        last_kernel,
        in_specs=[vmem] * 9,
        out_specs=[vmem] * 2,
        out_shape=[
            jax.ShapeDtypeStruct((count, width // 2), f32),
            jax.ShapeDtypeStruct((count, width // 2), bf16),
        ],
        compiler_params=grant(16),
        name="last",
    )(*parts, *weights, earlier)


def turned(array, axis, by):
    count = lax.axis_size(axis)
    return lax.ppermute(array, axis, [(i, (i + by) % count) for i in range(count)])


def body(
    tokens,
    in_gain,
    w_query,
    w_forget,
    w_input,
    w_outgate,
    w_conv_h,
    w_conv_b,
    w_conv_c,
    forget_floor,
    forget_leak,
    state_gain,
    conv_taps,
    group_gain,
    out_state,
    out_conv,
):
    x, c = lax.axis_index("x"), lax.axis_index("c")
    y, z = lax.axis_index("y"), lax.axis_index("z")
    here_y = y.astype(jnp.int32).reshape(1)
    here_z = z.astype(jnp.int32).reshape(1)
    first = ((y == 0) & (z == 0)).astype(jnp.int32).reshape(1)
    chips = lax.axis_size("x")
    width = tokens.shape[1] // chips
    gain_row = in_gain.reshape(1, -1)

    normed, keys, values, cums, message = front(
        tokens, gain_row, w_forget, w_input, forget_floor.reshape(1, -1), forget_leak
    )
    rim = turned(tokens[-16:], ("z", "y"), 1)
    near = [turned(message, "y", d) for d in (1, 2, 3)]

    def columns_for(chip):
        def cut(rows):
            mine = lax.dynamic_slice_in_dim(rows, chip * width + c * (width // 2), width // 2, 1)
            other = lax.dynamic_slice_in_dim(rows, chip * width + (1 - c) * (width // 2), width // 2, 1)
            return jnp.concatenate([mine, other], axis=1)

        return jnp.concatenate([cut(out_state), cut(out_conv)], axis=0)

    columns = [columns_for(x)] + [turned(columns_for((x + d) % chips), "x", d) for d in (1, 2, 3)]

    row_total, row_before, row_fade = join(row_kernel, here_y, message, *near)
    far = [turned(row_total, "z", d) for d in (1, 2, 3)]
    conv_res = conv(
        first, normed, rim, gain_row, w_conv_h, w_conv_c, w_conv_b, conv_taps, group_gain.reshape(1, -1)
    )
    window, column_before, column_fade = join(column_kernel, here_z, row_total, *far)
    farthest = turned(window, "z", 4)
    conv_all = [conv_res] + [turned(conv_res, "x", d) for d in (1, 2, 3)]
    reads, carries, gates = read(
        normed, w_query, w_outgate, state_gain.reshape(1, -1), keys, values, cums
    )
    state_res = finish(
        here_z, farthest, column_before, column_fade, row_before, row_fade, carries, reads, gates
    )
    state_all = [state_res] + [turned(state_res, "x", d) for d in (1, 2, 3)]
    half = project_half(conv_all, columns)
    kept, sent = project_last(state_all, columns, half)
    return (kept + turned(sent, "c", 1).astype(f32)).astype(bf16)


def solution(mesh):
    chips = 4
    rows = 4
    split = Mesh(
        mesh.devices.reshape(mesh.shape["sp"] // rows, rows, chips, mesh.shape["tp"] // chips),
        ("z", "y", "x", "c"),
    )
    sp, tp = ("z", "y"), ("x", "c")
    placed = (
        P(sp, None),
        P(),
        P(None, tp),
        P(None, tp),
        P(None, tp),
        P(None, tp),
        P(None, tp),
        P(None, tp),
        P(None, tp),
        P(tp),
        P(sp, tp),
        P(),
        P(None, tp),
        P(),
        P(tp, None),
        P(tp, None),
    )
    return jax.shard_map(body, mesh=split, in_specs=placed, out_specs=P(sp, tp), check_vma=False)
```

profile of v0, /device:TPU:1, one launch (start us, length us, event | category | flops | bytes accessed | tf_op | source)
XLA Modules:
  0.0 96.5 jit_solution(3567961519250901083)
XLA Ops:
  0.0 2.0 %constant_dynamic-slice_fusion.1 = (bf16[128,256]{1,0:T(8,128)(2,1)S(1)}, bf16[128,256]{1,0:T(8,128)(2,1)S(1)}, bf16[128,256]{1,0:T(8,128)(2,1)S(1)}, bf16[128,2...) fusion(bf16[128,2048]{1,0:T(8,128)(2,1)} %param.31, ...), kind=kLoop, calls=%fused_computation.6 | loop fusion | bytes 2097184 | tf_op jit(solution)/shard_map/dynamic_slice | solution.py:412
  2.1 2.1 %collective-permute-start.10 = (bf16[256,512]{1,0:T(8,128)(2,1)S(1)}, bf16[256,512]{1,0:T(8,128)(2,1)S(1)}, u32[]{:S(2)}, u32[]{:S(2)}) collective-permute-start(bf16[256,512]{1,0:T(8,128)(2,1)S(1)} %maximum_maximum_fusion.1), channel_id=1, source_target_pairs={{0,2},{2,4},{4,6},{6,0},{1,3},{3,5},{5,7},{7,1},{8,10},{10,12},{12... | collective-permute-start | bytes 786440 | tf_op jit(solution)/shard_map/ppermute | solution.py:374
  4.2 2.5 %collective-permute-start.11 = (bf16[256,512]{1,0:T(8,128)(2,1)S(1)}, bf16[256,512]{1,0:T(8,128)(2,1)S(1)}, u32[]{:S(2)}, u32[]{:S(2)}) collective-permute-start(bf16[256,512]{1,0:T(8,128)(2,1)S(1)} %maximum_maximum_fusion.2), channel_id=1, source_target_pairs={{0,4},{2,6},{4,0},{6,2},{1,5},{3,7},{5,1},{7,3},{8,12},{10,14},{12... | collective-permute-start | bytes 786440 | tf_op jit(solution)/shard_map/ppermute | solution.py:374
  11.4 8.9 %front.1 = (bf16[1024,2048]{1,0:T(8,128)(2,1)}, f32[1024,128]{1,0:T(8,128)}, bf16[1024,128]{1,0:T(8,128)(2,1)}, f32[1024,128]{1,0:T(8,128)}, bf16[144,128]{1,0:T(8,128)(2,1)}) custom-call(bf16[1024,2048]{1,0:T(8,128)(2,1)} %tokens.1, f32[1,2048]{1,0:T(1,128)} %bitcast.7, bf16[2048,128]{1,0:T(8,128)(2,1)} %w_forget.1, bf16[2048,128]{1,0:T(8,128)(2,1)} %w_input.1, ...), custom_call_target="tpu_custom_call" | custom-call | tf_op jit(solution)/shard_map/front/pallas_call | solution.py:96
  20.3 2.2 %copy-done = bf16[1024,2048]{1,0:T(8,128)(2,1)S(1)} copy-done((bf16[1024,2048]{1,0:T(8,128)(2,1)S(1)}, bf16[1024,2048]{1,0:T(8,128)(2,1)}, u32[]{:S(2)}) %copy-start) | copy-done | bytes 4194328
  22.5 3.8 %conv.1.refs_0_ = bf16[1024,128]{1,0:T(8,128)(2,1)S(1)} custom-call(s32[1]{0:T(128)} %bitcast.5.first, bf16[1024,2048]{1,0:T(8,128)(2,1)S(1)} %copy-done, bf16[16,2048]{1,0:T(8,128)(2,1)S(1)} %collective-permute-done.13.rim, f32[1,2048]{1,0:T(1,128)S(1)} %bitcast.8, bf16[2048,128]{1,0:T(8,128)(2,1)S(1)} %copy-done.2, bf16[2048,128]{1,0:T(8,128)(2,1)S(1)} %copy-done.3, ...), custom_call_target="tpu_custom_call" | custom-call | tf_op jit(solution)/shard_map/conv/pallas_call | solution.py:230
  28.0 2.8 %collective-permute-done.one = bf16[144,128]{1,0:T(8,128)(2,1)S(1)} collective-permute-done((bf16[144,128]{1,0:T(8,128)(2,1)S(1)}, bf16[144,128]{1,0:T(8,128)(2,1)S(1)}, u32[]{:S(2)}, u32[]{:S(2)}) %collective-permute-start) | collective-permute-done | bytes 36896 | tf_op jit(solution)/shard_map/ppermute | solution.py:374
  32.1 3.0 %collective-permute-done.1.two = bf16[144,128]{1,0:T(8,128)(2,1)S(1)} collective-permute-done((bf16[144,128]{1,0:T(8,128)(2,1)S(1)}, bf16[144,128]{1,0:T(8,128)(2,1)S(1)}, u32[]{:S(2)}, u32[]{:S(2)}) %collective-permute-start.1) | collective-permute-done | bytes 36896 | tf_op jit(solution)/shard_map/ppermute | solution.py:374
  35.1 1.5 %collective-permute-start.2 = (bf16[144,128]{1,0:T(8,128)(2,1)S(1)}, bf16[144,128]{1,0:T(8,128)(2,1)S(1)}, u32[]{:S(2)}, u32[]{:S(2)}) collective-permute-start(bf16[144,128]{1,0:T(8,128)(2,1)S(1)} %copy-done.10), channel_id=1, source_target_pairs={{0,24},{8,0},{16,8},{24,16},{1,25},{9,1},{17,9},{25,17},{2,26},{10... | collective-permute-start | bytes 110600 | tf_op jit(solution)/shard_map/ppermute | solution.py:374
  36.6 2.0 %collective-permute-done.2.three = bf16[144,128]{1,0:T(8,128)(2,1)S(1)} collective-permute-done((bf16[144,128]{1,0:T(8,128)(2,1)S(1)}, bf16[144,128]{1,0:T(8,128)(2,1)S(1)}, u32[]{:S(2)}, u32[]{:S(2)}) %collective-permute-start.2) | collective-permute-done | bytes 36896 | tf_op jit(solution)/shard_map/ppermute | solution.py:374
  38.6 1.7 %collective-permute-start.3 = (bf16[144,128]{1,0:T(8,128)(2,1)S(1)}, bf16[144,128]{1,0:T(8,128)(2,1)S(1)}, u32[]{:S(2)}, u32[]{:S(2)}) collective-permute-start(bf16[144,128]{1,0:T(8,128)(2,1)S(1)} %get-tuple-element.22.own), channel_id=1, source_target_pairs={{0,32},{32,64},{64,96},{96,128},{128,160},{160,192},{192,224},{224... | collective-permute-start | bytes 110600 | tf_op jit(solution)/shard_map/ppermute | solution.py:374
  40.4 4.9 %collective-permute-done.3.one = bf16[144,128]{1,0:T(8,128)(2,1)S(1)} collective-permute-done((bf16[144,128]{1,0:T(8,128)(2,1)S(1)}, bf16[144,128]{1,0:T(8,128)(2,1)S(1)}, u32[]{:S(2)}, u32[]{:S(2)}) %collective-permute-start.3) | collective-permute-done | bytes 36896 | tf_op jit(solution)/shard_map/ppermute | solution.py:374
  45.6 4.9 %collective-permute-done.4.two = bf16[144,128]{1,0:T(8,128)(2,1)S(1)} collective-permute-done((bf16[144,128]{1,0:T(8,128)(2,1)S(1)}, bf16[144,128]{1,0:T(8,128)(2,1)S(1)}, u32[]{:S(2)}, u32[]{:S(2)}) %collective-permute-start.4) | collective-permute-done | bytes 36896 | tf_op jit(solution)/shard_map/ppermute | solution.py:374
  51.2 5.8 %collective-permute-done.5.three = bf16[144,128]{1,0:T(8,128)(2,1)S(1)} collective-permute-done((bf16[144,128]{1,0:T(8,128)(2,1)S(1)}, bf16[144,128]{1,0:T(8,128)(2,1)S(1)}, u32[]{:S(2)}, u32[]{:S(2)}) %collective-permute-start.5) | collective-permute-done | bytes 36896 | tf_op jit(solution)/shard_map/ppermute | solution.py:374
  57.1 3.5 %collective-permute-start.6 = (bf16[144,128]{1,0:T(8,128)(2,1)S(1)}, bf16[144,128]{1,0:T(8,128)(2,1)S(1)}, u32[]{:S(2)}, u32[]{:S(2)}) collective-permute-start(bf16[144,128]{1,0:T(8,128)(2,1)S(1)} %get-tuple-element.23), channel_id=1, source_target_pairs={{0,128},{32,160},{64,192},{96,224},{128,0},{160,32},{192,64},{224,... | collective-permute-start | bytes 110600 | tf_op jit(solution)/shard_map/ppermute | solution.py:374
  60.6 5.4 %read.1 = (f32[1024,128]{1,0:T(8,128)S(1)}, bf16[1024,128]{1,0:T(8,128)(2,1)S(1)}, f32[1024,128]{1,0:T(8,128)S(1)}) custom-call(bf16[1024,2048]{1,0:T(8,128)(2,1)S(1)} %copy-done.1, bf16[2048,128]{1,0:T(8,128)(2,1)S(1)} %copy-done.5, bf16[2048,128]{1,0:T(8,128)(2,1)S(1)} %copy-done.6, f32[1,128]{1,0:T(1,128)S(1)} %bitcast.10, f32[1024,128]{1,0:T(8,128)S(1)} %copy-done.7, ...), custom_call_target="tpu_custom_call" | custom-call | tf_op jit(solution)/shard_map/read/pallas_call | solution.py:172
  67.3 1.7 %collective-permute-start.16 = (bf16[1024,128]{1,0:T(8,128)(2,1)S(1)}, bf16[1024,128]{1,0:T(8,128)(2,1)S(1)}, u32[]{:S(2)}, u32[]{:S(2)}) collective-permute-start(bf16[1024,128]{1,0:T(8,128)(2,1)S(1)} %conv.1.refs_0_), channel_id=1, source_target_pairs={{0,6},{2,0},{4,2},{6,4},{1,7},{3,1},{5,3},{7,5},{8,14},{10,8},{12,... | collective-permute-start | bytes 786440 | tf_op jit(solution)/shard_map/ppermute | solution.py:374
  69.6 1.8 %collective-permute-start.8 = (bf16[1024,128]{1,0:T(8,128)(2,1)S(1)}, bf16[1024,128]{1,0:T(8,128)(2,1)S(1)}, u32[]{:S(2)}, u32[]{:S(2)}) collective-permute-start(bf16[1024,128]{1,0:T(8,128)(2,1)S(1)} %finish.1.refs_0_), channel_id=1, source_target_pairs={{0,4},{2,6},{4,0},{6,2},{1,5},{3,7},{5,1},{7,3},{8,12},{10,14},{12... | collective-permute-start | bytes 786440 | tf_op jit(solution)/shard_map/ppermute | solution.py:374
  71.4 2.0 %collective-permute-start.9 = (bf16[1024,128]{1,0:T(8,128)(2,1)S(1)}, bf16[1024,128]{1,0:T(8,128)(2,1)S(1)}, u32[]{:S(2)}, u32[]{:S(2)}) collective-permute-start(bf16[1024,128]{1,0:T(8,128)(2,1)S(1)} %finish.1.refs_0_), channel_id=1, source_target_pairs={{0,6},{2,0},{4,2},{6,4},{1,7},{3,1},{5,3},{7,5},{8,14},{10,8},{12,... | collective-permute-start | bytes 786440 | tf_op jit(solution)/shard_map/ppermute | solution.py:374
  73.4 2.2 %collective-permute-done.16.refs_3_ = bf16[1024,128]{1,0:T(8,128)(2,1)S(1)} collective-permute-done((bf16[1024,128]{1,0:T(8,128)(2,1)S(1)}, bf16[1024,128]{1,0:T(8,128)(2,1)S(1)}, u32[]{:S(2)}, u32[]{:S(2)}) %collective-permute-start.16) | collective-permute-done | bytes 262176 | tf_op jit(solution)/shard_map/ppermute | solution.py:374
  76.4 2.1 %collective-permute-done.8.refs_2_ = bf16[1024,128]{1,0:T(8,128)(2,1)S(1)} collective-permute-done((bf16[1024,128]{1,0:T(8,128)(2,1)S(1)}, bf16[1024,128]{1,0:T(8,128)(2,1)S(1)}, u32[]{:S(2)}, u32[]{:S(2)}) %collective-permute-start.8) | collective-permute-done | bytes 262176 | tf_op jit(solution)/shard_map/ppermute | solution.py:374
  78.5 6.1 %collective-permute-done.9.refs_3_ = bf16[1024,128]{1,0:T(8,128)(2,1)S(1)} collective-permute-done((bf16[1024,128]{1,0:T(8,128)(2,1)S(1)}, bf16[1024,128]{1,0:T(8,128)(2,1)S(1)}, u32[]{:S(2)}, u32[]{:S(2)}) %collective-permute-start.9) | collective-permute-done | bytes 262176 | tf_op jit(solution)/shard_map/ppermute | solution.py:374
  85.3 8.8 %collective-permute-start.17 = (bf16[1024,256]{1,0:T(8,128)(2,1)S(1)}, bf16[1024,256]{1,0:T(8,128)(2,1)S(1)}, u32[]{:S(2)}, u32[]{:S(2)}) collective-permute-start(bf16[1024,256]{1,0:T(8,128)(2,1)S(1)} %get-tuple-element.36), channel_id=1, source_target_pairs={{0,1},{1,0},{2,3},{3,2},{4,5},{5,4},{6,7},{7,6},{8,9},{9,8},{10,11... | collective-permute-start | bytes 1572872 | tf_op jit(solution)/shard_map/ppermute | solution.py:374
  94.1 1.5 %collective-permute-done.17 = bf16[1024,256]{1,0:T(8,128)(2,1)S(1)} collective-permute-done((bf16[1024,256]{1,0:T(8,128)(2,1)S(1)}, bf16[1024,256]{1,0:T(8,128)(2,1)S(1)}, u32[]{:S(2)}, u32[]{:S(2)}) %collective-permute-start.17) | collective-permute-done | bytes 524320 | tf_op jit(solution)/shard_map/ppermute | solution.py:374
  (63 shorter events, 13.2 us)
Async XLA Ops:
  2.1 65.3 %collective-permute-start.10 = (bf16[256,512]{1,0:T(8,128)(2,1)S(1)}, bf16[256,512]{1,0:T(8,128)(2,1)S(1)}, u32[]{:S(2)}, u32[]{:S(2)}) collective-permute-start(bf16[256,512]{1,0:T(8,128)(2,1)S(1)} %maximum_maximum_fusion.1), channel_id=1, source_target_pairs={{0,2},{2,4},{4,6},{6,0},{1,3},{3,5},{5,7},{7,1},{8,10},{10,12},{12... | collective-permute-start | bytes 786440 | tf_op jit(solution)/shard_map/ppermute | solution.py:374
  4.2 64.8 %collective-permute-start.11 = (bf16[256,512]{1,0:T(8,128)(2,1)S(1)}, bf16[256,512]{1,0:T(8,128)(2,1)S(1)}, u32[]{:S(2)}, u32[]{:S(2)}) collective-permute-start(bf16[256,512]{1,0:T(8,128)(2,1)S(1)} %maximum_maximum_fusion.2), channel_id=1, source_target_pairs={{0,4},{2,6},{4,0},{6,2},{1,5},{3,7},{5,1},{7,3},{8,12},{10,14},{12... | collective-permute-start | bytes 786440 | tf_op jit(solution)/shard_map/ppermute | solution.py:374
  8.2 12.1 %collective-permute-start.13 = (bf16[16,2048]{1,0:T(8,128)(2,1)}, bf16[16,2048]{1,0:T(8,128)(2,1)S(1)}, u32[]{:S(2)}, u32[]{:S(2)}) collective-permute-start(bf16[16,2048]{1,0:T(8,128)(2,1)} %slice.3), channel_id=1, source_target_pairs={{0,8},{8,16},{16,24},{24,32},{32,40},{40,48},{48,56},{56,64},{64,7... | collective-permute-start | bytes 196616 | tf_op jit(solution)/shard_map/ppermute | solution.py:374
  10.2 59.4 %collective-permute-start.12 = (bf16[256,512]{1,0:T(8,128)(2,1)}, bf16[256,512]{1,0:T(8,128)(2,1)S(1)}, u32[]{:S(2)}, u32[]{:S(2)}) collective-permute-start(bf16[256,512]{1,0:T(8,128)(2,1)} %maximum_maximum_fusion.3), channel_id=1, source_target_pairs={{0,6},{2,0},{4,2},{6,4},{1,7},{3,1},{5,3},{7,5},{8,14},{10,8},{12,... | collective-permute-start | bytes 786440 | tf_op jit(solution)/shard_map/ppermute | solution.py:374
  11.4 49.2 %copy-start.5 = (bf16[2048,128]{1,0:T(8,128)(2,1)S(1)}, bf16[2048,128]{1,0:T(8,128)(2,1)}, u32[]{:S(2)}) copy-start(bf16[2048,128]{1,0:T(8,128)(2,1)} %w_query.1) | copy-start | bytes 1572868
  11.4 49.2 %copy-start.6 = (bf16[2048,128]{1,0:T(8,128)(2,1)S(1)}, bf16[2048,128]{1,0:T(8,128)(2,1)}, u32[]{:S(2)}) copy-start(bf16[2048,128]{1,0:T(8,128)(2,1)} %w_outgate.1) | copy-start | bytes 1572868
  20.3 40.4 %copy-start.14 = (f32[128]{0:T(128)S(1)}, f32[128]{0:T(128)}, u32[]{:S(2)}) copy-start(f32[128]{0:T(128)} %param.27) | copy-start | bytes 1540
  22.5 38.1 %copy-start.7 = (f32[1024,128]{1,0:T(8,128)S(1)}, f32[1024,128]{1,0:T(8,128)}, u32[]{:S(2)}) copy-start(f32[1024,128]{1,0:T(8,128)} %get-tuple-element.29.keys) | copy-start | bytes 1572868
  22.5 38.1 %copy-start.8 = (f32[1024,128]{1,0:T(8,128)S(1)}, f32[1024,128]{1,0:T(8,128)}, u32[]{:S(2)}) copy-start(f32[1024,128]{1,0:T(8,128)} %get-tuple-element.31.cums) | copy-start | bytes 1572868
  22.5 38.1 %copy-start.9 = (bf16[1024,128]{1,0:T(8,128)(2,1)S(1)}, bf16[1024,128]{1,0:T(8,128)(2,1)}, u32[]{:S(2)}) copy-start(bf16[1024,128]{1,0:T(8,128)(2,1)} %get-tuple-element.30.values) | copy-start | bytes 786436
  26.3 45.1 %collective-permute-start.14 = (bf16[1024,128]{1,0:T(8,128)(2,1)S(1)}, bf16[1024,128]{1,0:T(8,128)(2,1)S(1)}, u32[]{:S(2)}, u32[]{:S(2)}) collective-permute-start(bf16[1024,128]{1,0:T(8,128)(2,1)S(1)} %conv.1.refs_0_), channel_id=1, source_target_pairs={{0,2},{2,4},{4,6},{6,0},{1,3},{3,5},{5,7},{7,1},{8,10},{10,12},{12... | collective-permute-start | bytes 786440 | tf_op jit(solution)/shard_map/ppermute | solution.py:374
  26.7 4.1 %collective-permute-start = (bf16[144,128]{1,0:T(8,128)(2,1)S(1)}, bf16[144,128]{1,0:T(8,128)(2,1)S(1)}, u32[]{:S(2)}, u32[]{:S(2)}) collective-permute-start(bf16[144,128]{1,0:T(8,128)(2,1)S(1)} %copy-done.10), channel_id=1, source_target_pairs={{0,8},{8,16},{16,24},{24,0},{1,9},{9,17},{17,25},{25,1},{2,10},{10... | collective-permute-start | bytes 110600 | tf_op jit(solution)/shard_map/ppermute | solution.py:374
  30.8 4.3 %collective-permute-start.1 = (bf16[144,128]{1,0:T(8,128)(2,1)S(1)}, bf16[144,128]{1,0:T(8,128)(2,1)S(1)}, u32[]{:S(2)}, u32[]{:S(2)}) collective-permute-start(bf16[144,128]{1,0:T(8,128)(2,1)S(1)} %copy-done.10), channel_id=1, source_target_pairs={{0,16},{8,24},{16,0},{24,8},{1,17},{9,25},{17,1},{25,9},{2,18},{10... | collective-permute-start | bytes 110600 | tf_op jit(solution)/shard_map/ppermute | solution.py:374
  35.1 3.4 %collective-permute-start.2 = (bf16[144,128]{1,0:T(8,128)(2,1)S(1)}, bf16[144,128]{1,0:T(8,128)(2,1)S(1)}, u32[]{:S(2)}, u32[]{:S(2)}) collective-permute-start(bf16[144,128]{1,0:T(8,128)(2,1)S(1)} %copy-done.10), channel_id=1, source_target_pairs={{0,24},{8,0},{16,8},{24,16},{1,25},{9,1},{17,9},{25,17},{2,26},{10... | collective-permute-start | bytes 110600 | tf_op jit(solution)/shard_map/ppermute | solution.py:374
  38.6 6.6 %collective-permute-start.3 = (bf16[144,128]{1,0:T(8,128)(2,1)S(1)}, bf16[144,128]{1,0:T(8,128)(2,1)S(1)}, u32[]{:S(2)}, u32[]{:S(2)}) collective-permute-start(bf16[144,128]{1,0:T(8,128)(2,1)S(1)} %get-tuple-element.22.own), channel_id=1, source_target_pairs={{0,32},{32,64},{64,96},{96,128},{128,160},{160,192},{192,224},{224... | collective-permute-start | bytes 110600 | tf_op jit(solution)/shard_map/ppermute | solution.py:374
  45.2 5.3 %collective-permute-start.4 = (bf16[144,128]{1,0:T(8,128)(2,1)S(1)}, bf16[144,128]{1,0:T(8,128)(2,1)S(1)}, u32[]{:S(2)}, u32[]{:S(2)}) collective-permute-start(bf16[144,128]{1,0:T(8,128)(2,1)S(1)} %get-tuple-element.22.own), channel_id=1, source_target_pairs={{0,64},{32,96},{64,128},{96,160},{128,192},{160,224},{192,0},{224,... | collective-permute-start | bytes 110600 | tf_op jit(solution)/shard_map/ppermute | solution.py:374
  50.5 6.4 %collective-permute-start.5 = (bf16[144,128]{1,0:T(8,128)(2,1)S(1)}, bf16[144,128]{1,0:T(8,128)(2,1)S(1)}, u32[]{:S(2)}, u32[]{:S(2)}) collective-permute-start(bf16[144,128]{1,0:T(8,128)(2,1)S(1)} %get-tuple-element.22.own), channel_id=1, source_target_pairs={{0,96},{32,128},{64,160},{96,192},{128,224},{160,0},{192,32},{224,... | collective-permute-start | bytes 110600 | tf_op jit(solution)/shard_map/ppermute | solution.py:374
  57.1 9.0 %collective-permute-start.6 = (bf16[144,128]{1,0:T(8,128)(2,1)S(1)}, bf16[144,128]{1,0:T(8,128)(2,1)S(1)}, u32[]{:S(2)}, u32[]{:S(2)}) collective-permute-start(bf16[144,128]{1,0:T(8,128)(2,1)S(1)} %get-tuple-element.23), channel_id=1, source_target_pairs={{0,128},{32,160},{64,192},{96,224},{128,0},{160,32},{192,64},{224,... | collective-permute-start | bytes 110600 | tf_op jit(solution)/shard_map/ppermute | solution.py:374
  66.0 7.4 %collective-permute-start.15 = (bf16[1024,128]{1,0:T(8,128)(2,1)S(1)}, bf16[1024,128]{1,0:T(8,128)(2,1)S(1)}, u32[]{:S(2)}, u32[]{:S(2)}) collective-permute-start(bf16[1024,128]{1,0:T(8,128)(2,1)S(1)} %conv.1.refs_0_), channel_id=1, source_target_pairs={{0,4},{2,6},{4,0},{6,2},{1,5},{3,7},{5,1},{7,3},{8,12},{10,14},{12... | collective-permute-start | bytes 786440 | tf_op jit(solution)/shard_map/ppermute | solution.py:374
  67.3 8.3 %collective-permute-start.16 = (bf16[1024,128]{1,0:T(8,128)(2,1)S(1)}, bf16[1024,128]{1,0:T(8,128)(2,1)S(1)}, u32[]{:S(2)}, u32[]{:S(2)}) collective-permute-start(bf16[1024,128]{1,0:T(8,128)(2,1)S(1)} %conv.1.refs_0_), channel_id=1, source_target_pairs={{0,6},{2,0},{4,2},{6,4},{1,7},{3,1},{5,3},{7,5},{8,14},{10,8},{12,... | collective-permute-start | bytes 786440 | tf_op jit(solution)/shard_map/ppermute | solution.py:374
  69.0 7.3 %collective-permute-start.7 = (bf16[1024,128]{1,0:T(8,128)(2,1)S(1)}, bf16[1024,128]{1,0:T(8,128)(2,1)S(1)}, u32[]{:S(2)}, u32[]{:S(2)}) collective-permute-start(bf16[1024,128]{1,0:T(8,128)(2,1)S(1)} %finish.1.refs_0_), channel_id=1, source_target_pairs={{0,2},{2,4},{4,6},{6,0},{1,3},{3,5},{5,7},{7,1},{8,10},{10,12},{12... | collective-permute-start | bytes 786440 | tf_op jit(solution)/shard_map/ppermute | solution.py:374
  69.6 8.8 %collective-permute-start.8 = (bf16[1024,128]{1,0:T(8,128)(2,1)S(1)}, bf16[1024,128]{1,0:T(8,128)(2,1)S(1)}, u32[]{:S(2)}, u32[]{:S(2)}) collective-permute-start(bf16[1024,128]{1,0:T(8,128)(2,1)S(1)} %finish.1.refs_0_), channel_id=1, source_target_pairs={{0,4},{2,6},{4,0},{6,2},{1,5},{3,7},{5,1},{7,3},{8,12},{10,14},{12... | collective-permute-start | bytes 786440 | tf_op jit(solution)/shard_map/ppermute | solution.py:374
  71.4 13.2 %collective-permute-start.9 = (bf16[1024,128]{1,0:T(8,128)(2,1)S(1)}, bf16[1024,128]{1,0:T(8,128)(2,1)S(1)}, u32[]{:S(2)}, u32[]{:S(2)}) collective-permute-start(bf16[1024,128]{1,0:T(8,128)(2,1)S(1)} %finish.1.refs_0_), channel_id=1, source_target_pairs={{0,6},{2,0},{4,2},{6,4},{1,7},{3,1},{5,3},{7,5},{8,14},{10,8},{12,... | collective-permute-start | bytes 786440 | tf_op jit(solution)/shard_map/ppermute | solution.py:374
  85.3 10.3 %collective-permute-start.17 = (bf16[1024,256]{1,0:T(8,128)(2,1)S(1)}, bf16[1024,256]{1,0:T(8,128)(2,1)S(1)}, u32[]{:S(2)}, u32[]{:S(2)}) collective-permute-start(bf16[1024,256]{1,0:T(8,128)(2,1)S(1)} %get-tuple-element.36), channel_id=1, source_target_pairs={{0,1},{1,0},{2,3},{3,2},{4,5},{5,4},{6,7},{7,6},{8,9},{9,8},{10,11... | collective-permute-start | bytes 1572872 | tf_op jit(solution)/shard_map/ppermute | solution.py:374
  (12 other events, 203.4 us)
where the time goes:
time: 96.8 us; the launch traced here: 96.5 us
  waiting for transfers between devices  35.3 us (36%)
  starting transfers between devices  33.6 us (35%)
  Pallas kernels  19.9 us (21%)
  local copies, waits for them, and re-layouts  5.69 us (6%)
  other arithmetic  1.71 us (2%)
    ppermute x18, waiting for transfers between devices, turned(): lax.ppermute(array, axis, [(i, (i + by) % count) for i in range(count)])  35.3 us
    ppermute x18, starting transfers between devices, turned(): lax.ppermute(array, axis, [(i, (i + by) % count) for i in range(count)])  33.6 us
    pallas_call x1, Pallas kernels, front(): pl.pallas_call(front_kernel, grid=(count // FRONT,), in_specs=[pl.BlockSp...  8.87 us
    pallas_call x1, Pallas kernels, read(): pl.pallas_call(read_kernel, grid=(count // STEP,), in_specs=[pl.BlockSpec...  5.36 us
    pallas_call x1, Pallas kernels, conv(): pl.pallas_call(conv_kernel, grid=(count // STEP,), in_specs=[pl.BlockSpec...  3.77 us
    unnamed x36, local copies, waits for them, and re-layouts  2.26 us
    dynamic_slice x1, local copies, waits for them, and re-layouts, cut(): lax.dynamic_slice_in_dim(rows, chip * width + c * (width // 2), width //...  1.98 us
  transfers between devices with their start and end apart: 18, of which 10 were waited for; matrix products, arithmetic and copies ran while one was open for 2% of the time, Pallas kernels for 20%

commit v1 on v0

v1 whole, which is shorter than its diff:
```python
import jax
import jax.numpy as jnp
from jax import lax
from jax.experimental import pallas as pl
from jax.experimental.pallas import tpu as pltpu
from jax.sharding import Mesh
from jax.sharding import PartitionSpec as P


F = 128
BLOCK = 64
TAPS = 3
STEP = 256
FRONT = 256
PACK = F + 16
EPS = 1e-06
f32 = jnp.float32
bf16 = jnp.bfloat16


def dot(a, b, dims=((1,), (0,))):
    return lax.dot_general(a, b, (dims, ((), ())), preferred_element_type=f32)


def rms(values, gain):
    return values * lax.rsqrt(jnp.mean(values * values, axis=-1, keepdims=True) + EPS) * gain


def silu(x):
    return x * jax.nn.sigmoid(x)


def put_message(ref, state, decay, rim):
    high = decay.astype(bf16)
    low = (decay - high.astype(f32)).astype(bf16)
    ref[:F] = state.astype(bf16)
    row = lax.broadcasted_iota(jnp.int32, (16, F), 0)
    tail = jnp.where(row == 0, high.astype(f32), jnp.where(row == 1, low.astype(f32), 0.0))
    tail = jnp.where(row == 2, rim[0:1], jnp.where(row == 3, rim[1:2], tail))
    ref[F:] = tail.astype(bf16)


def get_message(ref):
    tail = ref[F:].astype(f32)
    return ref[:F].astype(f32), tail[0:1] + tail[1:2]


def get_rim(ref):
    return ref[F:].astype(f32)[2:4]


def grant(mib, **more):
    return pltpu.CompilerParams(vmem_limit_bytes=mib * 2**20, **more)


def front_kernel(place, tokens_h, gain_h, wf_h, wi_h, wq_h, wg_h, wh_h, wc_h, wb_h, floor_h, leak_h,
                 taps_h, group_h, sgain_h, ostate_h, oconv_h,
                 message, keys, values, cums, heads, extra, own, one, two, three,
                 tokens, gain, weights, floor, leak, taps, group, sgain, ostate, oconv, window, sems):
    count = tokens.shape[0]
    width = ostate.shape[1]
    copies = []

    def bring(src, dst):
        copy = pltpu.make_async_copy(src, dst, sems.at[len(copies)])
        copy.start()
        copies.append(copy)
        return copy

    def rows(step):
        return pl.ds(step * FRONT, FRONT)

    got_gain = bring(gain_h, gain)
    got_tokens = [bring(tokens_h.at[rows(0)], tokens.at[rows(0)])]
    got_weights = [
        bring(w, weights.at[:, pl.ds(j * F, F)])
        for j, w in enumerate((wf_h, wi_h, wq_h, wg_h, wh_h, wc_h, wb_h))
    ]
    small = [bring(floor_h, floor), bring(leak_h, leak), bring(taps_h, taps), bring(group_h, group), bring(sgain_h, sgain)]
    for step in range(1, count // FRONT):
        got_tokens.append(bring(tokens_h.at[rows(step)], tokens.at[rows(step)]))
    last_copies = [bring(ostate_h, ostate), bring(oconv_h, oconv)]

    row = lax.broadcasted_iota(jnp.int32, (STEP, STEP), 0)
    col = lax.broadcasted_iota(jnp.int32, (STEP, STEP), 1)
    tri = jnp.where(row >= col, 1.0, 0.0).astype(bf16)
    state = jnp.zeros((F, F), f32)
    total = jnp.zeros((1, F), f32)
    window[:8] = jnp.zeros((8, F), f32)
    got_gain.wait()
    for step in range(count // FRONT):
        top = step * FRONT
        got_tokens[step].wait()
        n = rms(tokens[top : top + FRONT].astype(f32), gain[...]).astype(bf16)
        if step == 0:
            for copy in got_weights:
                copy.wait()
        found = dot(n, weights[...]).astype(bf16)
        if step == 0:
            for copy in small:
                copy.wait()
        value = found[:, F : 2 * F]
        values[top : top + FRONT] = value
        heads[top : top + FRONT] = found[:, 2 * F : 4 * F]
        gate = found[:, :F].astype(f32)
        key = (1.0 - floor[...]) * jax.nn.sigmoid(-gate)
        keys[top : top + FRONT] = key
        log_forget = jnp.log1p(-key) + leak[top : top + FRONT]
        high = log_forget.astype(bf16)
        rest = log_forget - high.astype(f32)
        mid = rest.astype(bf16)
        low = (rest - mid.astype(f32)).astype(bf16)
        for at in range(0, FRONT, STEP):
            part = slice(at, at + STEP)
            cum = dot(tri, high[part]) + dot(tri, mid[part]) + dot(tri, low[part])
            cums[top + at : top + at + STEP] = cum
            last = cum[STEP - 1 : STEP]
            fresh = dot(value[part], (key[part] * jnp.exp(last - cum)).astype(bf16), ((0,), (0,)))
            state = state * jnp.exp(last) + fresh
            total = total + last
        signal = (found[:, 4 * F : 5 * F].astype(f32) * found[:, 5 * F : 6 * F].astype(f32)).astype(bf16).astype(f32)
        window[8 + top : 8 + top + FRONT] = signal
        scale = taps[...].astype(f32)
        near = scale[0:1] * window[6 + top : 6 + top + FRONT]
        near = near + scale[1:2] * window[7 + top : 7 + top + FRONT]
        near = near + scale[2:3] * signal
        after = found[:, 6 * F :].astype(f32)
        result = rms(after * near, group[...]).astype(bf16)
        for buffer in (own, one, two, three):
            buffer[top : top + FRONT] = result
        if step == 0:
            extra[:16] = signal[:16]
            extra[16:32] = after[:16]
            extra[32:35] = scale
            extra[35:36] = group[...]
            extra[36:37] = sgain[...]
    put_message(message, state, jnp.exp(total), window[count + 6 : count + 8])
    for copy in last_copies:
        copy.wait()
    _, _, x, c = unpack_place(place)
    for d, buffer in enumerate((own, one, two, three)):
        chip = (x + d) & 3
        for j in range(4):
            core = c if j < 2 else 1 - c
            at = pl.multiple_of(chip * (width // 4) + core * (width // 8) + (j & 1) * F, F)
            buffer[count + 2 * j * F : count + (2 * j + 1) * F] = ostate[:, pl.ds(at, F)]
            buffer[count + (2 * j + 1) * F : count + (2 * j + 2) * F] = oconv[:, pl.ds(at, F)]


def unpack_place(place):
    code = place[0]
    return code >> 5, (code >> 3) & 3, (code >> 1) & 3, code & 1


def front(place, tokens, gain, w7, floor, leak, taps, group, sgain, ostate, oconv):
    count, width = tokens.shape
    hbm = pl.BlockSpec(memory_space=pltpu.HBM)
    vmem = pl.BlockSpec(memory_space=pltpu.VMEM)
    buffer = jax.ShapeDtypeStruct((count + 8 * F, F), bf16)
    arrays = (tokens, gain, *w7, floor, leak, taps, group, sgain, ostate, oconv)
    return pl.pallas_call(
        front_kernel,
        in_specs=[pl.BlockSpec(memory_space=pltpu.SMEM)] + [hbm] * len(arrays),
        out_specs=[vmem] * 10,
        out_shape=[
            jax.ShapeDtypeStruct((PACK, F), bf16),
            jax.ShapeDtypeStruct((count, F), f32),
            jax.ShapeDtypeStruct((count, F), bf16),
            jax.ShapeDtypeStruct((count, F), f32),
            jax.ShapeDtypeStruct((count, 2 * F), bf16),
            jax.ShapeDtypeStruct((40, F), f32),
        ]
        + [buffer] * 4,
        scratch_shapes=[
            pltpu.VMEM((count, width), bf16),
            pltpu.VMEM((1, width), f32),
            pltpu.VMEM((width, 7 * F), bf16),
            pltpu.VMEM((1, F), f32),
            pltpu.VMEM((count, F), f32),
            pltpu.VMEM((TAPS, F), bf16),
            pltpu.VMEM((1, F), f32),
            pltpu.VMEM((1, F), f32),
            pltpu.VMEM(ostate.shape, bf16),
            pltpu.VMEM(oconv.shape, bf16),
            pltpu.VMEM((count + 8, F), f32),
            pltpu.SemaphoreType.DMA((15 + count // FRONT,)),
        ],
        compiler_params=grant(36),
        name="front",
    )(place, *[pltpu.with_memory_space_constraint(a, pltpu.HBM) for a in arrays])


def read_kernel(heads, extra, keys, values, cums, reads, carries, gates):
    row = lax.broadcasted_iota(jnp.int32, (BLOCK, BLOCK), 0)
    col = lax.broadcasted_iota(jnp.int32, (BLOCK, BLOCK), 1)
    start = jnp.zeros((F, F), f32)
    before = jnp.zeros((1, F), f32)
    for at in range(0, heads.shape[0], BLOCK):
        part = slice(at, at + BLOCK)
        gates[part] = silu(heads[part, F:].astype(f32)) * extra[36:37]
        q = silu(heads[part, :F].astype(f32))
        k = keys[part]
        v = values[part]
        base = jnp.zeros((1, F), f32) if at % STEP == 0 else cums[at - 1 : at]
        edge = cums[at + BLOCK - 1 : at + BLOCK]
        c = cums[part] - base
        half = c[BLOCK // 2 - 1 : BLOCK // 2]
        last = edge - base
        scores = dot((q * jnp.exp(c - half)).astype(bf16), (k * jnp.exp(half - c)).astype(bf16), ((1,), (1,)))
        scores = jnp.where(row >= col, scores, 0.0).astype(bf16)
        faded = q * jnp.exp(c)
        reads[part] = dot(scores, v) + dot(faded.astype(bf16), start.astype(bf16), ((1,), (1,)))
        carries[part] = (faded * jnp.exp(before)).astype(bf16)
        fresh = dot(v, (k * jnp.exp(last - c)).astype(bf16), ((0,), (0,)))
        start = start * jnp.exp(last) + fresh
        before = before + last


def read(heads, extra, keys, values, cums):
    count = heads.shape[0]
    vmem = pl.BlockSpec(memory_space=pltpu.VMEM)
    return pl.pallas_call(
        read_kernel,
        in_specs=[vmem] * 5,
        out_specs=[vmem] * 3,
        out_shape=[
            jax.ShapeDtypeStruct((count, F), f32),
            jax.ShapeDtypeStruct((count, F), bf16),
            jax.ShapeDtypeStruct((count, F), f32),
        ],
        compiler_params=grant(12),
        name="read",
    )(heads, extra, keys, values, cums)


def row_kernel(place_ref, own, one, two, three, total, before, fade):
    _, y, _, _ = unpack_place(place_ref)
    parts = [get_message(r) for r in (own, one, two, three)]
    place = [jnp.where(y >= d, y - d, y - d + 4) for d in range(4)]
    whole, inside = 0.0, 0.0
    product, product_before = 1.0, 1.0
    for d, (state, decay) in enumerate(parts):
        later = jnp.ones_like(decay)
        between = jnp.ones_like(decay)
        for other, (_, factor) in enumerate(parts):
            if other == d:
                continue
            behind = place[other] > place[d]
            later = later * jnp.where(behind, factor, 1.0)
            between = between * jnp.where(behind & (place[other] < y), factor, 1.0)
        whole = whole + state * later
        inside = inside + state * jnp.where(place[d] < y, between, 0.0)
        product = product * decay
        product_before = product_before * jnp.where(place[d] < y, decay, 1.0)
    put_message(total, whole, product, get_rim(one))
    before[...] = inside
    fade[...] = jnp.broadcast_to(product_before, fade.shape)


def column_kernel(place_ref, own, one, two, three, window, before, fade):
    z, _, _, _ = unpack_place(place_ref)
    state, product = jnp.zeros((F, F), f32), jnp.ones((1, F), f32)
    for d, ref in ((3, three), (2, two), (1, one)):
        piece, decay = get_message(ref)
        decay = jnp.where(z >= d, decay, 1.0)
        state = state * decay + jnp.where(z >= d, piece, 0.0)
        product = product * decay
    piece, decay = get_message(own)
    put_message(window, state * decay + piece, product * decay, get_rim(one))
    before[...] = state
    fade[...] = jnp.broadcast_to(product, fade.shape)


def join(kernel, index, *messages):
    vmem = pl.BlockSpec(memory_space=pltpu.VMEM)
    return pl.pallas_call(
        kernel,
        in_specs=[pl.BlockSpec(memory_space=pltpu.SMEM)] + [vmem] * 4,
        out_specs=[vmem] * 3,
        out_shape=[
            jax.ShapeDtypeStruct((PACK, F), bf16),
            jax.ShapeDtypeStruct((F, F), f32),
            jax.ShapeDtypeStruct((8, F), f32),
        ],
        compiler_params=grant(4),
    )(index, *messages)


def finish_kernel(place, far, near, row_total, column, column_fade, row, row_fade, carries, reads, gates, extra,
                  result, window):
    z, y, _, _ = unpack_place(place)
    piece, _ = get_message(far)
    piece = jnp.where(z >= 4, piece, 0.0)
    incoming = (column[...] + piece * column_fade[0:1]) * row_fade[0:1] + row[...]
    count = reads.shape[0]
    found = reads[...] + dot(carries[...], incoming.astype(bf16), ((1,), (1,)))
    result[:count] = rms(found, gates[...]).astype(bf16)
    rim = jnp.where(y > 0, get_rim(row_total), jnp.where(z > 0, get_rim(near), 0.0))
    window[6:8] = rim
    window[8:] = extra[:16]
    total = extra[32:33] * window[6:22] + extra[33:34] * window[7:23] + extra[34:35] * window[8:24]
    result[count:] = rms(extra[16:32] * total, extra[35:36]).astype(bf16)


def finish(place, *arrays):
    vmem = pl.BlockSpec(memory_space=pltpu.VMEM)
    return pl.pallas_call(
        finish_kernel,
        in_specs=[pl.BlockSpec(memory_space=pltpu.SMEM)] + [vmem] * len(arrays),
        out_specs=vmem,
        out_shape=jax.ShapeDtypeStruct((arrays[8].shape[0] + 16, F), bf16),
        scratch_shapes=[pltpu.VMEM((24, F), f32)],
        compiler_params=grant(12),
        name="finish",
    )(place, *arrays)


def weight_rows(buffers, half):
    count = buffers[0].shape[0] - 8 * F
    at = [count + (2 * j + half) * F for j in range(4)]
    return jnp.concatenate(
        [jnp.concatenate([r[a : a + F] for a in at], axis=1) for r in buffers], axis=0
    )


def half_kernel(own, one, two, three, out):
    buffers = (own, one, two, three)
    count = out.shape[0]
    out[...] = dot(jnp.concatenate([r[:count] for r in buffers], axis=1), weight_rows(buffers, 1))


def last_kernel(*refs):
    parts, buffers, earlier, kept, sent = refs[:4], refs[4:8], refs[8], refs[9], refs[10]
    count, full = earlier.shape
    width = full // 2
    state = dot(jnp.concatenate([r[:count] for r in parts], axis=1), weight_rows(buffers, 0))
    total = earlier[...] + state
    kept[...] = total[:, :width]
    sent[...] = total[:, width:].astype(bf16)
    first = state[:16] + dot(jnp.concatenate([r[count:] for r in parts], axis=1), weight_rows(buffers, 1))
    kept[:16] = first[:, :width]
    sent[:16] = first[:, width:].astype(bf16)


def project_half(buffers):
    vmem = pl.BlockSpec(memory_space=pltpu.VMEM)
    return pl.pallas_call(
        half_kernel,
        in_specs=[vmem] * 4,
        out_specs=vmem,
        out_shape=jax.ShapeDtypeStruct((buffers[0].shape[0] - 8 * F, 4 * F), f32),
        compiler_params=grant(14),
        name="half",
    )(*buffers)


def project_last(parts, buffers, earlier):
    vmem = pl.BlockSpec(memory_space=pltpu.VMEM)
    count, width = earlier.shape
    return pl.pallas_call(
        last_kernel,
        in_specs=[vmem] * 9,
        out_specs=[vmem] * 2,
        out_shape=[
            jax.ShapeDtypeStruct((count, width // 2), f32),
            jax.ShapeDtypeStruct((count, width // 2), bf16),
        ],
        compiler_params=grant(16),
        name="last",
    )(*parts, *buffers, earlier)


def turned(array, axis, by):
    count = lax.axis_size(axis)
    return lax.ppermute(array, axis, [(i, (i + by) % count) for i in range(count)])


def body(
    tokens,
    in_gain,
    w_query,
    w_forget,
    w_input,
    w_outgate,
    w_conv_h,
    w_conv_b,
    w_conv_c,
    forget_floor,
    forget_leak,
    state_gain,
    conv_taps,
    group_gain,
    out_state,
    out_conv,
):
    code = (lax.axis_index("z") * 4 + lax.axis_index("y")) * 4 + lax.axis_index("x")
    place = (code * 2 + lax.axis_index("c")).astype(jnp.int32).reshape(1)
    line = lambda row: row.reshape(1, -1)
    message, keys, values, cums, heads, extra, *buffers = front(
        place,
        tokens,
        line(in_gain),
        (w_forget, w_input, w_query, w_outgate, w_conv_h, w_conv_c, w_conv_b),
        line(forget_floor),
        forget_leak,
        conv_taps,
        line(group_gain),
        line(state_gain),
        out_state,
        out_conv,
    )
    near = [turned(message, "y", d) for d in (1, 2, 3)]
    buffers = buffers[:1] + [turned(buffers[d], "x", d) for d in (1, 2, 3)]
    row_total, row_before, row_fade = join(row_kernel, place, message, *near)
    far = [turned(row_total, "z", d) for d in (1, 2, 3)]
    reads, carries, gates = read(heads, extra, keys, values, cums)
    window, column_before, column_fade = join(column_kernel, place, row_total, *far)
    farthest = turned(window, "z", 4)
    state_res = finish(
        place, farthest, far[0], row_total, column_before, column_fade, row_before, row_fade,
        carries, reads, gates, extra,
    )
    state_all = [state_res] + [turned(state_res, "x", d) for d in (1, 2, 3)]
    half = project_half(buffers)
    kept, sent = project_last(state_all, buffers, half)
    return (kept + turned(sent, "c", 1).astype(f32)).astype(bf16)


def solution(mesh):
    chips = 4
    rows = 4
    split = Mesh(
        mesh.devices.reshape(mesh.shape["sp"] // rows, rows, chips, mesh.shape["tp"] // chips),
        ("z", "y", "x", "c"),
    )
    sp, tp = ("z", "y"), ("x", "c")
    placed = (
        P(sp, None),
        P(),
        P(None, tp),
        P(None, tp),
        P(None, tp),
        P(None, tp),
        P(None, tp),
        P(None, tp),
        P(None, tp),
        P(tp),
        P(sp, tp),
        P(),
        P(None, tp),
        P(),
        P(tp, None),
        P(tp, None),
    )
    return jax.shard_map(body, mesh=split, in_specs=placed, out_specs=P(sp, tp), check_vma=False)
```

time: 96.8 us -> 64.2 us (0.66)
  waiting for transfers between devices: 35.3 us -> 17.3 us
  Pallas kernels: 19.9 us -> 13.8 us
  local copies, waits for them, and re-layouts: 5.69 us -> 0 us
  starting transfers between devices: 33.6 us -> 32.1 us
    ppermute x18 -> x14, waiting for transfers between devices: 35.3 us -> 17.3 us  [turned(): lax.ppermute(array, axis, [(i, (i + by) % count) for i in range(count)])]
    pallas_call x4 -> x3, Pallas kernels: 18.7 us -> 12.5 us  [the longest x1 10.1 us: front(): pl.pallas_call(front_kernel, in_specs=[pl.BlockSpec(memory_space=pltpu.SM...]
    unnamed x36 -> x0, local copies, waits for them, and re-layouts: 2.26 us -> none
    dynamic_slice x1 -> x0, local copies, waits for them, and re-layouts: 1.98 us -> none  [cut(): lax.dynamic_slice_in_dim(rows, chip * width + c * (width // 2), width //...]
    ppermute x18 -> x14, starting transfers between devices: 33.6 us -> 32.1 us  [turned(): lax.ppermute(array, axis, [(i, (i + by) % count) for i in range(count)])]
    slice x1 -> x0, local copies, waits for them, and re-layouts: 1.46 us -> none  [body(): rim = turned(tokens[-16:], ('z', 'y'), 1)]
  transfers between devices with their start and end apart: 18 -> 14, of which waited for: 10 -> 10; matrix products, arithmetic and copies ran while one was open for 2% -> 0% of each run, Pallas kernels for 20% -> 5%
where the time goes in v1:
time: 64.2 us; the launch traced here: 64.1 us
  starting transfers between devices  32.1 us (50%)
  waiting for transfers between devices  17.3 us (27%)
  Pallas kernels  13.8 us (21%)
  other arithmetic  0.91 us (1%)
    ppermute x14, starting transfers between devices, turned(): lax.ppermute(array, axis, [(i, (i + by) % count) for i in range(count)])  32.1 us
    ppermute x14, waiting for transfers between devices, turned(): lax.ppermute(array, axis, [(i, (i + by) % count) for i in range(count)])  17.3 us
    pallas_call x1, Pallas kernels, front(): pl.pallas_call(front_kernel, in_specs=[pl.BlockSpec(memory_space=pltpu.SM...  10.1 us
    pallas_call x1, Pallas kernels, read(): pl.pallas_call(read_kernel, in_specs=[vmem] * 5, out_specs=[vmem] * 3, ou...  1.65 us
  transfers between devices with their start and end apart: 14, of which 10 were waited for; matrix products, arithmetic and copies ran while one was open for 0% of the time, Pallas kernels for 5%

profile of v1, /device:TPU:1, one launch (start us, length us, event | category | flops | bytes accessed | tf_op | source)
XLA Modules:
  0.0 64.1 jit_solution(18023241048954584957)
XLA Ops:
  0.0 10.1 %front.1 = (bf16[144,128]{1,0:T(8,128)(2,1)S(1)}, f32[1024,128]{1,0:T(8,128)S(1)}, bf16[1024,128]{1,0:T(8,128)(2,1)S(1)}, f32[1024,128]{1,0:T(8,128)S(1)}, bf16[...) custom-call(s32[1]{0:T(128)} %bitcast.place.place_ref, ...), custom_call_target="tpu_custom_call" | custom-call | tf_op jit(solution)/shard_map/front/pallas_call | solution.py:161
  10.1 2.1 %collective-permute-start.10 = (bf16[2048,128]{1,0:T(8,128)(2,1)S(1)}, bf16[2048,128]{1,0:T(8,128)(2,1)S(1)}, u32[]{:S(2)}, u32[]{:S(2)}) collective-permute-start(bf16[2048,128]{1,0:T(8,128)(2,1)S(1)} %get-tuple-element.42), channel_id=1, source_target_pairs={{0,2},{2,4},{4,6},{6,0},{1,3},{3,5},{5,7},{7,1},{8,10},{10,12},{12... | collective-permute-start | bytes 1572872 | tf_op jit(solution)/shard_map/ppermute | solution.py:375
  12.3 2.4 %collective-permute-start.11 = (bf16[2048,128]{1,0:T(8,128)(2,1)S(1)}, bf16[2048,128]{1,0:T(8,128)(2,1)S(1)}, u32[]{:S(2)}, u32[]{:S(2)}) collective-permute-start(bf16[2048,128]{1,0:T(8,128)(2,1)S(1)} %get-tuple-element.43), channel_id=1, source_target_pairs={{0,4},{2,6},{4,0},{6,2},{1,5},{3,7},{5,1},{7,3},{8,12},{10,14},{12... | collective-permute-start | bytes 1572872 | tf_op jit(solution)/shard_map/ppermute | solution.py:375
  14.7 1.2 %collective-permute-start.12 = (bf16[2048,128]{1,0:T(8,128)(2,1)S(1)}, bf16[2048,128]{1,0:T(8,128)(2,1)S(1)}, u32[]{:S(2)}, u32[]{:S(2)}) collective-permute-start(bf16[2048,128]{1,0:T(8,128)(2,1)S(1)} %get-tuple-element.44), channel_id=1, source_target_pairs={{0,6},{2,0},{4,2},{6,4},{1,7},{3,1},{5,3},{7,5},{8,14},{10,8},{12,... | collective-permute-start | bytes 1572872 | tf_op jit(solution)/shard_map/ppermute | solution.py:375
  15.9 2.7 %collective-permute-start.2 = (bf16[144,128]{1,0:T(8,128)(2,1)S(1)}, bf16[144,128]{1,0:T(8,128)(2,1)S(1)}, u32[]{:S(2)}, u32[]{:S(2)}) collective-permute-start(bf16[144,128]{1,0:T(8,128)(2,1)S(1)} %get-tuple-element.26.own), channel_id=1, source_target_pairs={{0,24},{8,0},{16,8},{24,16},{1,25},{9,1},{17,9},{25,17},{2,26},{10... | collective-permute-start | bytes 110600 | tf_op jit(solution)/shard_map/ppermute | solution.py:375
  18.9 0.7 %collective-permute-done.2.three = bf16[144,128]{1,0:T(8,128)(2,1)S(1)} collective-permute-done((bf16[144,128]{1,0:T(8,128)(2,1)S(1)}, bf16[144,128]{1,0:T(8,128)(2,1)S(1)}, u32[]{:S(2)}, u32[]{:S(2)}) %collective-permute-start.2) | collective-permute-done | bytes 36896 | tf_op jit(solution)/shard_map/ppermute | solution.py:375
  20.2 2.7 %collective-permute-done.1.two = bf16[144,128]{1,0:T(8,128)(2,1)S(1)} collective-permute-done((bf16[144,128]{1,0:T(8,128)(2,1)S(1)}, bf16[144,128]{1,0:T(8,128)(2,1)S(1)}, u32[]{:S(2)}, u32[]{:S(2)}) %collective-permute-start.1) | collective-permute-done | bytes 36896 | tf_op jit(solution)/shard_map/ppermute | solution.py:375
  22.9 1.6 %collective-permute-done.one = bf16[144,128]{1,0:T(8,128)(2,1)S(1)} collective-permute-done((bf16[144,128]{1,0:T(8,128)(2,1)S(1)}, bf16[144,128]{1,0:T(8,128)(2,1)S(1)}, u32[]{:S(2)}, u32[]{:S(2)}) %collective-permute-start) | collective-permute-done | bytes 36896 | tf_op jit(solution)/shard_map/ppermute | solution.py:375
  24.6 4.4 %collective-permute-start.5 = (bf16[144,128]{1,0:T(8,128)(2,1)S(1)}, bf16[144,128]{1,0:T(8,128)(2,1)S(1)}, u32[]{:S(2)}, u32[]{:S(2)}) collective-permute-start(bf16[144,128]{1,0:T(8,128)(2,1)S(1)} %get-tuple-element.27.own.row_total), channel_id=1, source_target_pairs={{0,96},{32,128},{64,160},{96,192},{128,224},{160,0},{192,32},{224,... | collective-permute-start | bytes 110600 | tf_op jit(solution)/shard_map/ppermute | solution.py:375
  29.0 3.3 %collective-permute-start.4 = (bf16[144,128]{1,0:T(8,128)(2,1)S(1)}, bf16[144,128]{1,0:T(8,128)(2,1)S(1)}, u32[]{:S(2)}, u32[]{:S(2)}) collective-permute-start(bf16[144,128]{1,0:T(8,128)(2,1)S(1)} %get-tuple-element.27.own.row_total), channel_id=1, source_target_pairs={{0,64},{32,96},{64,128},{96,160},{128,192},{160,224},{192,0},{224,... | collective-permute-start | bytes 110600 | tf_op jit(solution)/shard_map/ppermute | solution.py:375
  32.5 0.7 %collective-permute-start.3 = (bf16[144,128]{1,0:T(8,128)(2,1)S(1)}, bf16[144,128]{1,0:T(8,128)(2,1)S(1)}, u32[]{:S(2)}, u32[]{:S(2)}) collective-permute-start(bf16[144,128]{1,0:T(8,128)(2,1)S(1)} %get-tuple-element.27.own.row_total), channel_id=1, source_target_pairs={{0,32},{32,64},{64,96},{96,128},{128,160},{160,192},{192,224},{224... | collective-permute-start | bytes 110600 | tf_op jit(solution)/shard_map/ppermute | solution.py:375
  33.2 1.8 %collective-permute-done.4.two = bf16[144,128]{1,0:T(8,128)(2,1)S(1)} collective-permute-done((bf16[144,128]{1,0:T(8,128)(2,1)S(1)}, bf16[144,128]{1,0:T(8,128)(2,1)S(1)}, u32[]{:S(2)}, u32[]{:S(2)}) %collective-permute-start.4) | collective-permute-done | bytes 36896 | tf_op jit(solution)/shard_map/ppermute | solution.py:375
  35.0 1.8 %collective-permute-done.3.one.near = bf16[144,128]{1,0:T(8,128)(2,1)S(1)} collective-permute-done((bf16[144,128]{1,0:T(8,128)(2,1)S(1)}, bf16[144,128]{1,0:T(8,128)(2,1)S(1)}, u32[]{:S(2)}, u32[]{:S(2)}) %collective-permute-start.3) | collective-permute-done | bytes 36896 | tf_op jit(solution)/shard_map/ppermute | solution.py:375
  36.9 5.5 %collective-permute-start.6 = (bf16[144,128]{1,0:T(8,128)(2,1)S(1)}, bf16[144,128]{1,0:T(8,128)(2,1)S(1)}, u32[]{:S(2)}, u32[]{:S(2)}) collective-permute-start(bf16[144,128]{1,0:T(8,128)(2,1)S(1)} %get-tuple-element.28), channel_id=1, source_target_pairs={{0,128},{32,160},{64,192},{96,224},{128,0},{160,32},{192,64},{224,... | collective-permute-start | bytes 110600 | tf_op jit(solution)/shard_map/ppermute | solution.py:375
  42.4 1.7 %read.1 = (f32[1024,128]{1,0:T(8,128)S(1)}, bf16[1024,128]{1,0:T(8,128)(2,1)S(1)}, f32[1024,128]{1,0:T(8,128)S(1)}) custom-call(bf16[1024,256]{1,0:T(8,128)(2,1)S(1)} %get-tuple-element.33.heads, f32[40,128]{1,0:T(8,128)S(1)} %get-tuple-element.34.extra, f32[1024,128]{1,0:T(8,128)S(1)} %get-tuple-element.35.keys, ...), custom_call_target="tpu_custom_call" | custom-call | tf_op jit(solution)/shard_map/read/pallas_call | solution.py:222
  44.6 2.0 %collective-permute-start.8 = (bf16[1040,128]{1,0:T(8,128)(2,1)S(1)}, bf16[1040,128]{1,0:T(8,128)(2,1)S(1)}, u32[]{:S(2)}, u32[]{:S(2)}) collective-permute-start(bf16[1040,128]{1,0:T(8,128)(2,1)S(1)} %finish.1.refs_0_), channel_id=1, source_target_pairs={{0,4},{2,6},{4,0},{6,2},{1,5},{3,7},{5,1},{7,3},{8,12},{10,14},{12... | collective-permute-start | bytes 798728 | tf_op jit(solution)/shard_map/ppermute | solution.py:375
  46.6 0.7 %half.1.refs_8_ = f32[1024,512]{1,0:T(8,128)S(1)} custom-call(bf16[2048,128]{1,0:T(8,128)(2,1)S(1)} %get-tuple-element.41.own.refs_4_, bf16[2048,128]{1,0:T(8,128)(2,1)S(1)} %collective-permute-done.10.one.refs_5_, bf16[2048,128]{1,0:T(8,128)(2,1)S(1)} %collective-permute-done.11.two.refs_6_, bf16[2048,128]{1,0:T(8,128)(2,1)S(1)} %collective-permute-done.12.three.refs_7_), custom_call_target="tpu_custom_call" | custom-call | tf_op jit(solution)/shard_map/half/pallas_call | solution.py:347
  47.3 2.5 %collective-permute-done.9.refs_3_ = bf16[1040,128]{1,0:T(8,128)(2,1)S(1)} collective-permute-done((bf16[1040,128]{1,0:T(8,128)(2,1)S(1)}, bf16[1040,128]{1,0:T(8,128)(2,1)S(1)}, u32[]{:S(2)}, u32[]{:S(2)}) %collective-permute-start.9) | collective-permute-done | bytes 266272 | tf_op jit(solution)/shard_map/ppermute | solution.py:375
  49.8 1.7 %collective-permute-done.8.refs_2_ = bf16[1040,128]{1,0:T(8,128)(2,1)S(1)} collective-permute-done((bf16[1040,128]{1,0:T(8,128)(2,1)S(1)}, bf16[1040,128]{1,0:T(8,128)(2,1)S(1)}, u32[]{:S(2)}, u32[]{:S(2)}) %collective-permute-start.8) | collective-permute-done | bytes 266272 | tf_op jit(solution)/shard_map/ppermute | solution.py:375
  51.5 2.8 %collective-permute-done.7.refs_1_ = bf16[1040,128]{1,0:T(8,128)(2,1)S(1)} collective-permute-done((bf16[1040,128]{1,0:T(8,128)(2,1)S(1)}, bf16[1040,128]{1,0:T(8,128)(2,1)S(1)}, u32[]{:S(2)}, u32[]{:S(2)}) %collective-permute-start.7) | collective-permute-done | bytes 266272 | tf_op jit(solution)/shard_map/ppermute | solution.py:375
  54.3 0.8 %last.1 = (f32[1024,256]{1,0:T(8,128)S(1)}, bf16[1024,256]{1,0:T(8,128)(2,1)S(1)}) custom-call(bf16[1040,128]{1,0:T(8,128)(2,1)S(1)} %finish.1.refs_0_, bf16[1040,128]{1,0:T(8,128)(2,1)S(1)} %collective-permute-done.7.refs_1_, bf16[1040,128]{1,0:T(8,128)(2,1)S(1)} %collective-permute-done.8.refs_2_, bf16[1040,128]{1,0:T(8,128)(2,1)S(1)} %collective-permute-done.9.refs_3_, ...), custom_call_target="tpu_custom_call" | custom-call | tf_op jit(solution)/shard_map/last/pallas_call | solution.py:360
  55.0 6.7 %collective-permute-start.13 = (bf16[1024,256]{1,0:T(8,128)(2,1)S(1)}, bf16[1024,256]{1,0:T(8,128)(2,1)S(1)}, u32[]{:S(2)}, u32[]{:S(2)}) collective-permute-start(bf16[1024,256]{1,0:T(8,128)(2,1)S(1)} %get-tuple-element.46), channel_id=1, source_target_pairs={{0,1},{1,0},{2,3},{3,2},{4,5},{5,4},{6,7},{7,6},{8,9},{9,8},{10,11... | collective-permute-start | bytes 1572872 | tf_op jit(solution)/shard_map/ppermute | solution.py:375
  61.7 1.5 %collective-permute-done.13 = bf16[1024,256]{1,0:T(8,128)(2,1)S(1)} collective-permute-done((bf16[1024,256]{1,0:T(8,128)(2,1)S(1)}, bf16[1024,256]{1,0:T(8,128)(2,1)S(1)}, u32[]{:S(2)}, u32[]{:S(2)}) %collective-permute-start.13) | collective-permute-done | bytes 524320 | tf_op jit(solution)/shard_map/ppermute | solution.py:375
  63.2 0.9 %add_convert_fusion = bf16[1024,256]{1,0:T(8,128)(2,1)} fusion(f32[1024,256]{1,0:T(8,128)S(1)} %get-tuple-element.45, bf16[1024,256]{1,0:T(8,128)(2,1)S(1)} %collective-permute-done.13), kind=kLoop, calls=%fused_computation | loop fusion | flops 786432 | bytes 2097152 | tf_op jit(solution)/shard_map/convert_element_type | solution.py:426
  (12 shorter events, 1.7 us)
Async XLA Ops:
  10.1 36.5 %collective-permute-start.10 = (bf16[2048,128]{1,0:T(8,128)(2,1)S(1)}, bf16[2048,128]{1,0:T(8,128)(2,1)S(1)}, u32[]{:S(2)}, u32[]{:S(2)}) collective-permute-start(bf16[2048,128]{1,0:T(8,128)(2,1)S(1)} %get-tuple-element.42), channel_id=1, source_target_pairs={{0,2},{2,4},{4,6},{6,0},{1,3},{3,5},{5,7},{7,1},{8,10},{10,12},{12... | collective-permute-start | bytes 1572872 | tf_op jit(solution)/shard_map/ppermute | solution.py:375
  12.3 34.3 %collective-permute-start.11 = (bf16[2048,128]{1,0:T(8,128)(2,1)S(1)}, bf16[2048,128]{1,0:T(8,128)(2,1)S(1)}, u32[]{:S(2)}, u32[]{:S(2)}) collective-permute-start(bf16[2048,128]{1,0:T(8,128)(2,1)S(1)} %get-tuple-element.43), channel_id=1, source_target_pairs={{0,4},{2,6},{4,0},{6,2},{1,5},{3,7},{5,1},{7,3},{8,12},{10,14},{12... | collective-permute-start | bytes 1572872 | tf_op jit(solution)/shard_map/ppermute | solution.py:375
  14.7 31.9 %collective-permute-start.12 = (bf16[2048,128]{1,0:T(8,128)(2,1)S(1)}, bf16[2048,128]{1,0:T(8,128)(2,1)S(1)}, u32[]{:S(2)}, u32[]{:S(2)}) collective-permute-start(bf16[2048,128]{1,0:T(8,128)(2,1)S(1)} %get-tuple-element.44), channel_id=1, source_target_pairs={{0,6},{2,0},{4,2},{6,4},{1,7},{3,1},{5,3},{7,5},{8,14},{10,8},{12,... | collective-permute-start | bytes 1572872 | tf_op jit(solution)/shard_map/ppermute | solution.py:375
  15.9 3.8 %collective-permute-start.2 = (bf16[144,128]{1,0:T(8,128)(2,1)S(1)}, bf16[144,128]{1,0:T(8,128)(2,1)S(1)}, u32[]{:S(2)}, u32[]{:S(2)}) collective-permute-start(bf16[144,128]{1,0:T(8,128)(2,1)S(1)} %get-tuple-element.26.own), channel_id=1, source_target_pairs={{0,24},{8,0},{16,8},{24,16},{1,25},{9,1},{17,9},{25,17},{2,26},{10... | collective-permute-start | bytes 110600 | tf_op jit(solution)/shard_map/ppermute | solution.py:375
  18.6 4.3 %collective-permute-start.1 = (bf16[144,128]{1,0:T(8,128)(2,1)S(1)}, bf16[144,128]{1,0:T(8,128)(2,1)S(1)}, u32[]{:S(2)}, u32[]{:S(2)}) collective-permute-start(bf16[144,128]{1,0:T(8,128)(2,1)S(1)} %get-tuple-element.26.own), channel_id=1, source_target_pairs={{0,16},{8,24},{16,0},{24,8},{1,17},{9,25},{17,1},{25,9},{2,18},{10... | collective-permute-start | bytes 110600 | tf_op jit(solution)/shard_map/ppermute | solution.py:375
  19.7 4.9 %collective-permute-start = (bf16[144,128]{1,0:T(8,128)(2,1)S(1)}, bf16[144,128]{1,0:T(8,128)(2,1)S(1)}, u32[]{:S(2)}, u32[]{:S(2)}) collective-permute-start(bf16[144,128]{1,0:T(8,128)(2,1)S(1)} %get-tuple-element.26.own), channel_id=1, source_target_pairs={{0,8},{8,16},{16,24},{24,0},{1,9},{9,17},{17,25},{25,1},{2,10},{10... | collective-permute-start | bytes 110600 | tf_op jit(solution)/shard_map/ppermute | solution.py:375
  24.6 7.9 %collective-permute-start.5 = (bf16[144,128]{1,0:T(8,128)(2,1)S(1)}, bf16[144,128]{1,0:T(8,128)(2,1)S(1)}, u32[]{:S(2)}, u32[]{:S(2)}) collective-permute-start(bf16[144,128]{1,0:T(8,128)(2,1)S(1)} %get-tuple-element.27.own.row_total), channel_id=1, source_target_pairs={{0,96},{32,128},{64,160},{96,192},{128,224},{160,0},{192,32},{224,... | collective-permute-start | bytes 110600 | tf_op jit(solution)/shard_map/ppermute | solution.py:375
  29.0 6.0 %collective-permute-start.4 = (bf16[144,128]{1,0:T(8,128)(2,1)S(1)}, bf16[144,128]{1,0:T(8,128)(2,1)S(1)}, u32[]{:S(2)}, u32[]{:S(2)}) collective-permute-start(bf16[144,128]{1,0:T(8,128)(2,1)S(1)} %get-tuple-element.27.own.row_total), channel_id=1, source_target_pairs={{0,64},{32,96},{64,128},{96,160},{128,192},{160,224},{192,0},{224,... | collective-permute-start | bytes 110600 | tf_op jit(solution)/shard_map/ppermute | solution.py:375
  32.5 4.3 %collective-permute-start.3 = (bf16[144,128]{1,0:T(8,128)(2,1)S(1)}, bf16[144,128]{1,0:T(8,128)(2,1)S(1)}, u32[]{:S(2)}, u32[]{:S(2)}) collective-permute-start(bf16[144,128]{1,0:T(8,128)(2,1)S(1)} %get-tuple-element.27.own.row_total), channel_id=1, source_target_pairs={{0,32},{32,64},{64,96},{96,128},{128,160},{160,192},{192,224},{224... | collective-permute-start | bytes 110600 | tf_op jit(solution)/shard_map/ppermute | solution.py:375
  36.9 7.1 %collective-permute-start.6 = (bf16[144,128]{1,0:T(8,128)(2,1)S(1)}, bf16[144,128]{1,0:T(8,128)(2,1)S(1)}, u32[]{:S(2)}, u32[]{:S(2)}) collective-permute-start(bf16[144,128]{1,0:T(8,128)(2,1)S(1)} %get-tuple-element.28), channel_id=1, source_target_pairs={{0,128},{32,160},{64,192},{96,224},{128,0},{160,32},{192,64},{224,... | collective-permute-start | bytes 110600 | tf_op jit(solution)/shard_map/ppermute | solution.py:375
  44.5 5.3 %collective-permute-start.9 = (bf16[1040,128]{1,0:T(8,128)(2,1)S(1)}, bf16[1040,128]{1,0:T(8,128)(2,1)S(1)}, u32[]{:S(2)}, u32[]{:S(2)}) collective-permute-start(bf16[1040,128]{1,0:T(8,128)(2,1)S(1)} %finish.1.refs_0_), channel_id=1, source_target_pairs={{0,6},{2,0},{4,2},{6,4},{1,7},{3,1},{5,3},{7,5},{8,14},{10,8},{12,... | collective-permute-start | bytes 798728 | tf_op jit(solution)/shard_map/ppermute | solution.py:375
  44.6 7.0 %collective-permute-start.8 = (bf16[1040,128]{1,0:T(8,128)(2,1)S(1)}, bf16[1040,128]{1,0:T(8,128)(2,1)S(1)}, u32[]{:S(2)}, u32[]{:S(2)}) collective-permute-start(bf16[1040,128]{1,0:T(8,128)(2,1)S(1)} %finish.1.refs_0_), channel_id=1, source_target_pairs={{0,4},{2,6},{4,0},{6,2},{1,5},{3,7},{5,1},{7,3},{8,12},{10,14},{12... | collective-permute-start | bytes 798728 | tf_op jit(solution)/shard_map/ppermute | solution.py:375
  46.6 7.7 %collective-permute-start.7 = (bf16[1040,128]{1,0:T(8,128)(2,1)S(1)}, bf16[1040,128]{1,0:T(8,128)(2,1)S(1)}, u32[]{:S(2)}, u32[]{:S(2)}) collective-permute-start(bf16[1040,128]{1,0:T(8,128)(2,1)S(1)} %finish.1.refs_0_), channel_id=1, source_target_pairs={{0,2},{2,4},{4,6},{6,0},{1,3},{3,5},{5,7},{7,1},{8,10},{10,12},{12... | collective-permute-start | bytes 798728 | tf_op jit(solution)/shard_map/ppermute | solution.py:375
  55.0 8.2 %collective-permute-start.13 = (bf16[1024,256]{1,0:T(8,128)(2,1)S(1)}, bf16[1024,256]{1,0:T(8,128)(2,1)S(1)}, u32[]{:S(2)}, u32[]{:S(2)}) collective-permute-start(bf16[1024,256]{1,0:T(8,128)(2,1)S(1)} %get-tuple-element.46), channel_id=1, source_target_pairs={{0,1},{1,0},{2,3},{3,2},{4,5},{5,4},{6,7},{7,6},{8,9},{9,8},{10,11... | collective-permute-start | bytes 1572872 | tf_op jit(solution)/shard_map/ppermute | solution.py:375

commit v2 on v1

v2 whole, which is shorter than its diff:
```python
import functools

import jax
import jax.numpy as jnp
from jax import lax
from jax.experimental import pallas as pl
from jax.experimental.pallas import tpu as pltpu
from jax.sharding import Mesh
from jax.sharding import PartitionSpec as P


F = 128
BLOCK = 64
STEP = 256
FRONT = 256
PACK = F + 16
EPS = 1e-06
ROWS = 8
f32 = jnp.float32
bf16 = jnp.bfloat16


def dot(a, b, dims=((1,), (0,))):
    return lax.dot_general(a, b, (dims, ((), ())), preferred_element_type=f32)


def rms(values, gain):
    return values * lax.rsqrt(jnp.mean(values * values, axis=-1, keepdims=True) + EPS) * gain


def silu(x):
    return x * jax.nn.sigmoid(x)


def put_message(ref, state, decay, rim):
    high = decay.astype(bf16)
    low = (decay - high.astype(f32)).astype(bf16)
    ref[:F] = state.astype(bf16)
    row = lax.broadcasted_iota(jnp.int32, (16, F), 0)
    tail = jnp.where(row == 0, high.astype(f32), jnp.where(row == 1, low.astype(f32), 0.0))
    tail = jnp.where(row == 2, rim[0:1], jnp.where(row == 3, rim[1:2], tail))
    ref[F:] = tail.astype(bf16)


def get_message(ref):
    tail = ref[F:].astype(f32)
    return ref[:F].astype(f32), tail[0:1] + tail[1:2]


def get_rim(ref):
    return ref[F:].astype(f32)[2:4]


def grant(mib, **more):
    return pltpu.CompilerParams(vmem_limit_bytes=mib * 2**20, **more)


def front_kernel(place, tokens_h, gain_h, wf_h, wi_h, wh_h, wc_h, wb_h, wq_h, wg_h, floor_h, leak_h,
                 ostate_h, oconv_h,
                 tokens, scales, message, keys, values, cums, later, own, one, two, three,
                 gain, weights, floor, leak, ostate, oconv, sems):
    count, width = tokens.shape
    copies = []

    def bring(src, dst):
        copy = pltpu.make_async_copy(src, dst, sems.at[len(copies)])
        copy.start()
        copies.append(copy)
        return copy

    got_gain = bring(gain_h, gain)
    half = FRONT // 2
    got_first = [bring(tokens_h.at[pl.ds(at, half)], tokens.at[pl.ds(at, half)]) for at in (0, half)]
    got_weights = [bring(w, weights.at[:, pl.ds(j * F, F)]) for j, w in enumerate((wf_h, wi_h))]
    others = [bring(floor_h, floor), bring(leak_h, leak)]
    others += [
        bring(tokens_h.at[pl.ds(at, FRONT)], tokens.at[pl.ds(at, FRONT)]) for at in range(FRONT, count, FRONT)
    ]
    last_copies = [bring(wh_h, later.at[:, pl.ds(0, F)]), bring(wc_h, later.at[:, pl.ds(F, F)])]
    last_copies += [bring(ostate_h, ostate), bring(oconv_h, oconv)]
    next_copies = [bring(w, later.at[:, pl.ds((2 + j) * F, F)]) for j, w in enumerate((wb_h, wq_h, wg_h))]

    row = lax.broadcasted_iota(jnp.int32, (STEP, STEP), 0)
    col = lax.broadcasted_iota(jnp.int32, (STEP, STEP), 1)
    tri = jnp.where(row >= col, 1.0, 0.0).astype(bf16)
    state = jnp.zeros((F, F), f32)
    total = jnp.zeros((1, F), f32)

    def norm(top, size):
        part = tokens[top : top + size].astype(f32)
        mean = jnp.mean(part * part, axis=-1, keepdims=True)
        scales[top : top + size] = jnp.broadcast_to(lax.rsqrt(mean + EPS), (size, F))
        tokens[top : top + size] = (part * gain[...]).astype(bf16)

    def project(top):
        scale = scales[top : top + FRONT]
        found = dot(tokens[top : top + FRONT], weights[...])
        return (found * jnp.concatenate([scale, scale], axis=1)).astype(bf16)

    def gates(top, found, state, total):
        value = found[:, F:]
        values[top : top + FRONT] = value
        gate = found[:, :F].astype(f32)
        key = (1.0 - floor[...]) * jax.nn.sigmoid(-gate)
        keys[top : top + FRONT] = key
        log_forget = jnp.log1p(-key) + leak[top : top + FRONT]
        high = log_forget.astype(bf16)
        rest = log_forget - high.astype(f32)
        mid = rest.astype(bf16)
        low = (rest - mid.astype(f32)).astype(bf16)
        for at in range(0, FRONT, STEP):
            part = slice(at, at + STEP)
            cum = dot(tri, high[part]) + dot(tri, mid[part]) + dot(tri, low[part])
            cums[top + at : top + at + STEP] = cum
            last = cum[STEP - 1 : STEP]
            fresh = dot(value[part], (key[part] * jnp.exp(last - cum)).astype(bf16), ((0,), (0,)))
            state = state * jnp.exp(last) + fresh
            total = total + last
        return state, total

    got_gain.wait()
    for copy, top in zip(got_first, (0, half)):
        copy.wait()
        norm(top, half)
    for copy in got_weights:
        copy.wait()
    found = project(0)
    for copy in others:
        copy.wait()
    for top in range(FRONT, count, FRONT):
        norm(top, FRONT)
        following = project(top)
        state, total = gates(top - FRONT, found, state, total)
        found = following
    for copy in last_copies:
        copy.wait()
    scale = scales[count - 16 :]
    edge = dot(tokens[count - 16 :], later[:, : 2 * F]) * jnp.concatenate([scale, scale], axis=1)
    edge = edge.astype(bf16).astype(f32)
    state, total = gates(count - FRONT, found, state, total)
    put_message(message, state, jnp.exp(total), (edge[:, :F] * edge[:, F:])[14:])
    _, _, x, c = unpack_place(place)
    for d, buffer in enumerate((own, one, two, three)):
        for j in range(4):
            core = c if j < 2 else 1 - c
            at = pl.multiple_of(((x + d) & 3) * (width // 4) + core * (width // 8) + (j & 1) * F, F)
            buffer[:F, j * F : (j + 1) * F] = ostate[:, pl.ds(at, F)]
            buffer[F:, j * F : (j + 1) * F] = oconv[:, pl.ds(at, F)]
    for copy in next_copies:
        copy.wait()


def unpack_place(place):
    code = place[0]
    return code >> 5, (code >> 3) & 3, (code >> 1) & 3, code & 1


def in_hbm(arrays):
    return [pltpu.with_memory_space_constraint(a, pltpu.HBM) for a in arrays]


def front(place, *arrays):
    count, width = arrays[0].shape
    ostate = arrays[-1]
    hbm = pl.BlockSpec(memory_space=pltpu.HBM)
    vmem = pl.BlockSpec(memory_space=pltpu.VMEM)
    return pl.pallas_call(
        front_kernel,
        in_specs=[pl.BlockSpec(memory_space=pltpu.SMEM)] + [hbm] * len(arrays),
        out_specs=[vmem] * 11,
        out_shape=[
            jax.ShapeDtypeStruct((count, width), bf16),
            jax.ShapeDtypeStruct((count, F), f32),
            jax.ShapeDtypeStruct((PACK, F), bf16),
            jax.ShapeDtypeStruct((count, F), f32),
            jax.ShapeDtypeStruct((count, F), bf16),
            jax.ShapeDtypeStruct((count, F), f32),
            jax.ShapeDtypeStruct((width, 5 * F), bf16),
        ]
        + [jax.ShapeDtypeStruct((2 * F, 4 * F), bf16)] * 4,
        scratch_shapes=[
            pltpu.VMEM((1, width), f32),
            pltpu.VMEM((width, 2 * F), bf16),
            pltpu.VMEM((1, F), f32),
            pltpu.VMEM((count, F), f32),
            pltpu.VMEM(ostate.shape, bf16),
            pltpu.VMEM(ostate.shape, bf16),
            pltpu.SemaphoreType.DMA((13 + count // FRONT,)),
        ],
        compiler_params=grant(24),
        name="front",
    )(place, *in_hbm(arrays))


def conv_kernel(normed, scales, weights, taps, group, sgain, heads, extra, result, window):
    count = normed.shape[0]
    window[:8] = jnp.zeros((8, F), f32)

    def project(top, first, last):
        found = dot(normed[top : top + FRONT], weights[:, first * F : last * F])
        return (found * jnp.concatenate([scales[top : top + FRONT]] * (last - first), axis=1)).astype(bf16)

    def convolve(top, found):
        signal = (found[:, :F].astype(f32) * found[:, F : 2 * F].astype(f32)).astype(bf16).astype(f32)
        window[8 + top : 8 + top + FRONT] = signal
        scale = taps[...].astype(f32)
        near = scale[0:1] * window[6 + top : 6 + top + FRONT]
        near = near + scale[1:2] * window[7 + top : 7 + top + FRONT]
        near = near + scale[2:3] * signal
        after = found[:, 2 * F :].astype(f32)
        result[top : top + FRONT] = rms(after * near, group[...]).astype(bf16)
        if top == 0:
            extra[:16] = signal[:16]
            extra[16:32] = after[:16]
            extra[32:35] = scale
            extra[35:36] = group[...]
            extra[36:37] = sgain[...]

    for top in range(0, count, FRONT):
        mixed = project(top, 0, 3)
        heads[top : top + FRONT] = project(top, 3, 5)
        convolve(top, mixed)


def conv(normed, *arrays):
    count, _ = normed.shape
    vmem = pl.BlockSpec(memory_space=pltpu.VMEM)
    return pl.pallas_call(
        conv_kernel,
        in_specs=[vmem] * 6,
        out_specs=[vmem] * 3,
        out_shape=[
            jax.ShapeDtypeStruct((count, 2 * F), bf16),
            jax.ShapeDtypeStruct((40, F), f32),
            jax.ShapeDtypeStruct((count, F), bf16),
        ],
        scratch_shapes=[pltpu.VMEM((count + 8, F), f32)],
        compiler_params=grant(16),
        name="conv",
    )(normed, *arrays)


def read_kernel(heads, extra, keys, values, cums, reads, carries, gates):
    row = lax.broadcasted_iota(jnp.int32, (BLOCK, BLOCK), 0)
    col = lax.broadcasted_iota(jnp.int32, (BLOCK, BLOCK), 1)
    start = jnp.zeros((F, F), f32)
    before = jnp.zeros((1, F), f32)
    for at in range(0, heads.shape[0], BLOCK):
        part = slice(at, at + BLOCK)
        gates[part] = silu(heads[part, F:].astype(f32)) * extra[36:37]
        q = silu(heads[part, :F].astype(f32))
        k = keys[part]
        v = values[part]
        base = jnp.zeros((1, F), f32) if at % STEP == 0 else cums[at - 1 : at]
        edge = cums[at + BLOCK - 1 : at + BLOCK]
        c = cums[part] - base
        half = c[BLOCK // 2 - 1 : BLOCK // 2]
        last = edge - base
        scores = dot((q * jnp.exp(c - half)).astype(bf16), (k * jnp.exp(half - c)).astype(bf16), ((1,), (1,)))
        scores = jnp.where(row >= col, scores, 0.0).astype(bf16)
        faded = q * jnp.exp(c)
        reads[part] = dot(scores, v) + dot(faded.astype(bf16), start.astype(bf16), ((1,), (1,)))
        carries[part] = (faded * jnp.exp(before)).astype(bf16)
        fresh = dot(v, (k * jnp.exp(last - c)).astype(bf16), ((0,), (0,)))
        start = start * jnp.exp(last) + fresh
        before = before + last


def read(heads, extra, keys, values, cums):
    count = heads.shape[0]
    vmem = pl.BlockSpec(memory_space=pltpu.VMEM)
    return pl.pallas_call(
        read_kernel,
        in_specs=[vmem] * 5,
        out_specs=[vmem] * 3,
        out_shape=[
            jax.ShapeDtypeStruct((count, F), f32),
            jax.ShapeDtypeStruct((count, F), bf16),
            jax.ShapeDtypeStruct((count, F), f32),
        ],
        compiler_params=grant(12),
        name="read",
    )(heads, extra, keys, values, cums)


def row_kernel(place_ref, own, one, two, three, total, before, fade):
    _, y, _, _ = unpack_place(place_ref)
    parts = [get_message(r) for r in (own, one, two, three)]
    place = [jnp.where(y >= d, y - d, y - d + 4) for d in range(4)]
    whole, inside = 0.0, 0.0
    product, product_before = 1.0, 1.0
    for d, (state, decay) in enumerate(parts):
        later = jnp.ones_like(decay)
        between = jnp.ones_like(decay)
        for other, (_, factor) in enumerate(parts):
            if other == d:
                continue
            behind = place[other] > place[d]
            later = later * jnp.where(behind, factor, 1.0)
            between = between * jnp.where(behind & (place[other] < y), factor, 1.0)
        whole = whole + state * later
        inside = inside + state * jnp.where(place[d] < y, between, 0.0)
        product = product * decay
        product_before = product_before * jnp.where(place[d] < y, decay, 1.0)
    put_message(total, whole, product, get_rim(one))
    before[...] = inside
    fade[...] = jnp.broadcast_to(product_before, fade.shape)


def column_kernel(place_ref, own, behind, ahead, window):
    z, _, _, _ = unpack_place(place_ref)
    state, decay = get_message(behind)
    state = jnp.where(z > 0, state, 0.0)
    decay = jnp.where(z > 0, decay, 1.0)
    piece, factor = get_message(own)
    state = state * factor + piece
    decay = decay * factor
    piece, factor = get_message(ahead)
    state = jnp.where(z == ROWS - 1, piece, state * factor + piece)
    decay = jnp.where(z == ROWS - 1, factor, decay * factor)
    put_message(window, state, decay, jnp.zeros((2, F), f32))


def column(place, *messages):
    vmem = pl.BlockSpec(memory_space=pltpu.VMEM)
    return pl.pallas_call(
        column_kernel,
        in_specs=[pl.BlockSpec(memory_space=pltpu.SMEM)] + [vmem] * 3,
        out_specs=vmem,
        out_shape=jax.ShapeDtypeStruct((PACK, F), bf16),
        compiler_params=grant(4),
        name="column",
    )(place, *messages)


def join(kernel, index, *messages):
    vmem = pl.BlockSpec(memory_space=pltpu.VMEM)
    return pl.pallas_call(
        kernel,
        in_specs=[pl.BlockSpec(memory_space=pltpu.SMEM)] + [vmem] * 4,
        out_specs=[vmem] * 3,
        out_shape=[
            jax.ShapeDtypeStruct((PACK, F), bf16),
            jax.ShapeDtypeStruct((F, F), f32),
            jax.ShapeDtypeStruct((8, F), f32),
        ],
        compiler_params=grant(4),
    )(index, *messages)


def finish_kernel(place, six, three, near, row_total, row, row_fade, carries, reads, gates, extra,
                  result, window):
    z, y, _, _ = unpack_place(place)
    incoming = jnp.zeros((F, F), f32)
    for ref, least in ((six, 5), (three, 2), (near, 1)):
        piece, decay = get_message(ref)
        incoming = jnp.where(z >= least, incoming * decay + piece, incoming)
    incoming = incoming * row_fade[0:1] + row[...]
    count = reads.shape[0]
    found = reads[...] + dot(carries[...], incoming.astype(bf16), ((1,), (1,)))
    result[:count] = rms(found, gates[...]).astype(bf16)
    rim = jnp.where(y > 0, get_rim(row_total), jnp.where(z > 0, get_rim(near), 0.0))
    window[6:8] = rim
    window[8:] = extra[:16]
    total = extra[32:33] * window[6:22] + extra[33:34] * window[7:23] + extra[34:35] * window[8:24]
    result[count:] = rms(extra[16:32] * total, extra[35:36]).astype(bf16)


def finish(place, *arrays):
    vmem = pl.BlockSpec(memory_space=pltpu.VMEM)
    return pl.pallas_call(
        finish_kernel,
        in_specs=[pl.BlockSpec(memory_space=pltpu.SMEM)] + [vmem] * len(arrays),
        out_specs=vmem,
        out_shape=jax.ShapeDtypeStruct((arrays[7].shape[0] + 16, F), bf16),
        scratch_shapes=[pltpu.VMEM((24, F), f32)],
        compiler_params=grant(12),
        name="finish",
    )(place, *arrays)


def half_kernel(*refs):
    parts, weights, out = refs[:4], refs[4:8], refs[8]
    out[...] = dot(
        jnp.concatenate([r[...] for r in parts], axis=1),
        jnp.concatenate([r[F:] for r in weights], axis=0),
    )


def last_kernel(mine, *refs):
    parts, weights, earlier, out = refs[:4], refs[4:8], refs[8], refs[9]
    count, width = out.shape
    at = slice(0, width) if mine else slice(width, 2 * width)
    state = dot(
        jnp.concatenate([r[:count] for r in parts], axis=1),
        jnp.concatenate([r[:F, at] for r in weights], axis=0),
    )
    first = state[:16] + dot(
        jnp.concatenate([r[count:] for r in parts], axis=1),
        jnp.concatenate([r[F:, at] for r in weights], axis=0),
    )
    out[16:] = (earlier[16:, at] + state[16:]).astype(out.dtype)
    out[:16] = first.astype(out.dtype)


def project_half(parts, weights):
    vmem = pl.BlockSpec(memory_space=pltpu.VMEM)
    return pl.pallas_call(
        half_kernel,
        in_specs=[vmem] * 8,
        out_specs=vmem,
        out_shape=jax.ShapeDtypeStruct((parts[0].shape[0], 4 * F), f32),
        compiler_params=grant(14),
        name="half",
    )(*parts, *weights)


def project_last(mine, parts, weights, earlier):
    vmem = pl.BlockSpec(memory_space=pltpu.VMEM)
    count, width = earlier.shape
    return pl.pallas_call(
        functools.partial(last_kernel, mine),
        in_specs=[vmem] * 9,
        out_specs=vmem,
        out_shape=jax.ShapeDtypeStruct((count, width // 2), f32 if mine else bf16),
        compiler_params=grant(14),
        name="kept" if mine else "sent",
    )(*parts, *weights, earlier)


def turned(array, axis, by):
    count = lax.axis_size(axis)
    return lax.ppermute(array, axis, [(i, (i + by) % count) for i in range(count)])


def body(
    tokens,
    in_gain,
    w_query,
    w_forget,
    w_input,
    w_outgate,
    w_conv_h,
    w_conv_b,
    w_conv_c,
    forget_floor,
    forget_leak,
    state_gain,
    conv_taps,
    group_gain,
    out_state,
    out_conv,
):
    code = (lax.axis_index("z") * 4 + lax.axis_index("y")) * 4 + lax.axis_index("x")
    place = (code * 2 + lax.axis_index("c")).astype(jnp.int32).reshape(1)
    line = lambda row: row.reshape(1, -1)
    normed, scales, message, keys, values, cums, later, *columns = front(
        place,
        tokens,
        line(in_gain),
        w_forget,
        w_input,
        w_conv_h,
        w_conv_c,
        w_conv_b,
        w_query,
        w_outgate,
        line(forget_floor),
        forget_leak,
        out_state,
        out_conv,
    )
    near = [turned(message, "y", d) for d in (1, 2, 3)]
    columns = columns[:1] + [turned(columns[d], "x", d) for d in (1, 2, 3)]
    heads, extra, conv_res = conv(
        normed, scales, later, conv_taps, line(group_gain), line(state_gain)
    )
    row_total, row_before, row_fade = join(row_kernel, place, message, *near)
    near = [turned(row_total, "z", d) for d in (1, ROWS - 1)]
    conv_all = [conv_res] + [turned(conv_res, "x", d) for d in (1, 2, 3)]
    reads, carries, gates = read(heads, extra, keys, values, cums)
    window = column(place, row_total, *near)
    three, six = [turned(window, "z", d) for d in (3, 6)]
    state_res = finish(
        place, six, three, near[0], row_total, row_before, row_fade, carries, reads, gates, extra
    )
    state_all = [state_res] + [turned(state_res, "x", d) for d in (1, 2, 3)]
    half = project_half(conv_all, columns)
    sent = project_last(False, state_all, columns, half)
    got = turned(sent, "c", 1)
    kept = project_last(True, state_all, columns, half)
    return (kept + got.astype(f32)).astype(bf16)


def solution(mesh):
    assert mesh.shape["sp"] == 4 * ROWS
    chips = 4
    rows = 4
    split = Mesh(
        mesh.devices.reshape(mesh.shape["sp"] // rows, rows, chips, mesh.shape["tp"] // chips),
        ("z", "y", "x", "c"),
    )
    sp, tp = ("z", "y"), ("x", "c")
    placed = (
        P(sp, None),
        P(),
        P(None, tp),
        P(None, tp),
        P(None, tp),
        P(None, tp),
        P(None, tp),
        P(None, tp),
        P(None, tp),
        P(tp),
        P(sp, tp),
        P(),
        P(None, tp),
        P(),
        P(tp, None),
        P(tp, None),
    )
    return jax.shard_map(body, mesh=split, in_specs=placed, out_specs=P(sp, tp), check_vma=False)
```

time: 64.2 us -> 79.7 us (1.24)
  waiting for transfers between devices: 17.3 us -> 34.4 us
  starting transfers between devices: 32.1 us -> 30.4 us
    ppermute x14 -> x17, waiting for transfers between devices: 17.3 us -> 34.4 us  [turned(): lax.ppermute(array, axis, [(i, (i + by) % count) for i in range(count)])]
    pallas_call x2 -> x5, Pallas kernels: 1.46 us -> 5.36 us  [the longest x1 3.71 us: conv(): pl.pallas_call(conv_kernel, in_specs=[vmem] * 6, out_specs=[vmem] * 3, ou...]
    pallas_call x1, Pallas kernels: 10.1 us -> 6.23 us  [front(): pl.pallas_call(front_kernel, in_specs=[pl.BlockSpec(memory_space=pltpu.SM...]
    ppermute x14 -> x17, starting transfers between devices: 32.1 us -> 30.4 us  [turned(): lax.ppermute(array, axis, [(i, (i + by) % count) for i in range(count)])]
  transfers between devices with their start and end apart: 14 -> 17, of which waited for: 10 -> 9; matrix products, arithmetic and copies ran while one was open for 0% -> 0% of each run, Pallas kernels for 5% -> 4%
where the time goes in v2:
time: 79.7 us; the launch traced here: 79.6 us
  waiting for transfers between devices  34.4 us (43%)
  starting transfers between devices  30.4 us (38%)
  Pallas kernels  13.7 us (17%)
  other arithmetic  0.95 us (1%)
    ppermute x17, waiting for transfers between devices, turned(): lax.ppermute(array, axis, [(i, (i + by) % count) for i in range(count)])  34.4 us
    ppermute x17, starting transfers between devices, turned(): lax.ppermute(array, axis, [(i, (i + by) % count) for i in range(count)])  30.4 us
    pallas_call x1, Pallas kernels, front(): pl.pallas_call(front_kernel, in_specs=[pl.BlockSpec(memory_space=pltpu.SM...  6.23 us
    pallas_call x1, Pallas kernels, conv(): pl.pallas_call(conv_kernel, in_specs=[vmem] * 6, out_specs=[vmem] * 3, ou...  3.71 us
    pallas_call x1, Pallas kernels, read(): pl.pallas_call(read_kernel, in_specs=[vmem] * 5, out_specs=[vmem] * 3, ou...  1.66 us
  transfers between devices with their start and end apart: 17, of which 9 were waited for; matrix products, arithmetic and copies ran while one was open for 0% of the time, Pallas kernels for 4%

profile of v2, /device:TPU:1, one launch (start us, length us, event | category | flops | bytes accessed | tf_op | source)
XLA Modules:
  0.0 79.6 jit_solution(4312457161785147558)
XLA Ops:
  0.0 6.2 %front.1 = (bf16[1024,2048]{1,0:T(8,128)(2,1)S(1)}, f32[1024,128]{1,0:T(8,128)S(1)}, bf16[144,128]{1,0:T(8,128)(2,1)S(1)}, f32[1024,128]{1,0:T(8,128)S(1)}, bf16...) custom-call(s32[1]{0:T(128)} %bitcast.place.place_ref, ...), custom_call_target="tpu_custom_call" | custom-call | tf_op jit(solution)/shard_map/front/pallas_call | solution.py:167
  6.3 3.7 %conv.1 = (bf16[1024,256]{1,0:T(8,128)(2,1)S(1)}, f32[40,128]{1,0:T(8,128)S(1)}, bf16[1024,128]{1,0:T(8,128)(2,1)S(1)}) custom-call(bf16[1024,2048]{1,0:T(8,128)(2,1)S(1)} %get-tuple-element.29.normed, f32[1024,128]{1,0:T(8,128)S(1)} %get-tuple-element.30.scales, bf16[2048,640]{1,0:T(8,128)(2,1)S(1)} %get-tuple-element.31.weights, ...), custom_call_target="tpu_custom_call" | custom-call | tf_op jit(solution)/shard_map/conv/pallas_call | solution.py:228
  10.0 3.4 %collective-permute-start.15 = (bf16[1024,128]{1,0:T(8,128)(2,1)S(1)}, bf16[1024,128]{1,0:T(8,128)(2,1)S(1)}, u32[]{:S(2)}, u32[]{:S(2)}) collective-permute-start(bf16[1024,128]{1,0:T(8,128)(2,1)S(1)} %get-tuple-element.44.refs_0_), channel_id=1, source_target_pairs={{0,6},{2,0},{4,2},{6,4},{1,7},{3,1},{5,3},{7,5},{8,14},{10,8},{12,... | collective-permute-start | bytes 786440 | tf_op jit(solution)/shard_map/ppermute | solution.py:433
  13.9 2.7 %collective-permute-start.2 = (bf16[144,128]{1,0:T(8,128)(2,1)S(1)}, bf16[144,128]{1,0:T(8,128)(2,1)S(1)}, u32[]{:S(2)}, u32[]{:S(2)}) collective-permute-start(bf16[144,128]{1,0:T(8,128)(2,1)S(1)} %get-tuple-element.25.own), channel_id=1, source_target_pairs={{0,24},{8,0},{16,8},{24,16},{1,25},{9,1},{17,9},{25,17},{2,26},{10... | collective-permute-start | bytes 110600 | tf_op jit(solution)/shard_map/ppermute | solution.py:433
  17.2 1.5 %collective-permute-start.10 = (bf16[256,512]{1,0:T(8,128)(2,1)S(1)}, bf16[256,512]{1,0:T(8,128)(2,1)S(1)}, u32[]{:S(2)}, u32[]{:S(2)}) collective-permute-start(bf16[256,512]{1,0:T(8,128)(2,1)S(1)} %get-tuple-element.41), channel_id=1, source_target_pairs={{0,2},{2,4},{4,6},{6,0},{1,3},{3,5},{5,7},{7,1},{8,10},{10,12},{12... | collective-permute-start | bytes 786440 | tf_op jit(solution)/shard_map/ppermute | solution.py:433
  18.8 1.1 %collective-permute-start.1 = (bf16[144,128]{1,0:T(8,128)(2,1)S(1)}, bf16[144,128]{1,0:T(8,128)(2,1)S(1)}, u32[]{:S(2)}, u32[]{:S(2)}) collective-permute-start(bf16[144,128]{1,0:T(8,128)(2,1)S(1)} %get-tuple-element.25.own), channel_id=1, source_target_pairs={{0,16},{8,24},{16,0},{24,8},{1,17},{9,25},{17,1},{25,9},{2,18},{10... | collective-permute-start | bytes 110600 | tf_op jit(solution)/shard_map/ppermute | solution.py:433
  19.9 3.5 %collective-permute-done.1.two = bf16[144,128]{1,0:T(8,128)(2,1)S(1)} collective-permute-done((bf16[144,128]{1,0:T(8,128)(2,1)S(1)}, bf16[144,128]{1,0:T(8,128)(2,1)S(1)}, u32[]{:S(2)}, u32[]{:S(2)}) %collective-permute-start.1) | collective-permute-done | bytes 36896 | tf_op jit(solution)/shard_map/ppermute | solution.py:433
  23.4 4.3 %collective-permute-done.one = bf16[144,128]{1,0:T(8,128)(2,1)S(1)} collective-permute-done((bf16[144,128]{1,0:T(8,128)(2,1)S(1)}, bf16[144,128]{1,0:T(8,128)(2,1)S(1)}, u32[]{:S(2)}, u32[]{:S(2)}) %collective-permute-start) | collective-permute-done | bytes 36896 | tf_op jit(solution)/shard_map/ppermute | solution.py:433
  27.8 5.6 %collective-permute-start.4 = (bf16[144,128]{1,0:T(8,128)(2,1)S(1)}, bf16[144,128]{1,0:T(8,128)(2,1)S(1)}, u32[]{:S(2)}, u32[]{:S(2)}) collective-permute-start(bf16[144,128]{1,0:T(8,128)(2,1)S(1)} %get-tuple-element.26.own.row_total), channel_id=1, source_target_pairs={{0,224},{32,0},{64,32},{96,64},{128,96},{160,128},{192,160},{224,1... | collective-permute-start | bytes 110600 | tf_op jit(solution)/shard_map/ppermute | solution.py:433
  33.4 1.1 %collective-permute-done.4.ahead = bf16[144,128]{1,0:T(8,128)(2,1)S(1)} collective-permute-done((bf16[144,128]{1,0:T(8,128)(2,1)S(1)}, bf16[144,128]{1,0:T(8,128)(2,1)S(1)}, u32[]{:S(2)}, u32[]{:S(2)}) %collective-permute-start.4) | collective-permute-done | bytes 36896 | tf_op jit(solution)/shard_map/ppermute | solution.py:433
  34.5 4.6 %collective-permute-done.3.behind.near = bf16[144,128]{1,0:T(8,128)(2,1)S(1)} collective-permute-done((bf16[144,128]{1,0:T(8,128)(2,1)S(1)}, bf16[144,128]{1,0:T(8,128)(2,1)S(1)}, u32[]{:S(2)}, u32[]{:S(2)}) %collective-permute-start.3) | collective-permute-done | bytes 36896 | tf_op jit(solution)/shard_map/ppermute | solution.py:433
  39.6 6.2 %collective-permute-done.6.three = bf16[144,128]{1,0:T(8,128)(2,1)S(1)} collective-permute-done((bf16[144,128]{1,0:T(8,128)(2,1)S(1)}, bf16[144,128]{1,0:T(8,128)(2,1)S(1)}, u32[]{:S(2)}, u32[]{:S(2)}) %collective-permute-start.6) | collective-permute-done | bytes 36896 | tf_op jit(solution)/shard_map/ppermute | solution.py:433
  46.1 1.7 %read.1 = (f32[1024,128]{1,0:T(8,128)S(1)}, bf16[1024,128]{1,0:T(8,128)(2,1)S(1)}, f32[1024,128]{1,0:T(8,128)S(1)}) custom-call(bf16[1024,256]{1,0:T(8,128)(2,1)S(1)} %get-tuple-element.32.heads, f32[40,128]{1,0:T(8,128)S(1)} %get-tuple-element.33.extra, f32[1024,128]{1,0:T(8,128)S(1)} %get-tuple-element.34.keys, ...), custom_call_target="tpu_custom_call" | custom-call | tf_op jit(solution)/shard_map/read/pallas_call | solution.py:272
  47.7 1.8 %collective-permute-done.5.six = bf16[144,128]{1,0:T(8,128)(2,1)S(1)} collective-permute-done((bf16[144,128]{1,0:T(8,128)(2,1)S(1)}, bf16[144,128]{1,0:T(8,128)(2,1)S(1)}, u32[]{:S(2)}, u32[]{:S(2)}) %collective-permute-start.5) | collective-permute-done | bytes 36896 | tf_op jit(solution)/shard_map/ppermute | solution.py:433
  49.9 1.0 %collective-permute-start.9 = (bf16[1040,128]{1,0:T(8,128)(2,1)S(1)}, bf16[1040,128]{1,0:T(8,128)(2,1)S(1)}, u32[]{:S(2)}, u32[]{:S(2)}) collective-permute-start(bf16[1040,128]{1,0:T(8,128)(2,1)S(1)} %finish.1.refs_0_), channel_id=1, source_target_pairs={{0,6},{2,0},{4,2},{6,4},{1,7},{3,1},{5,3},{7,5},{8,14},{10,8},{12,... | collective-permute-start | bytes 798728 | tf_op jit(solution)/shard_map/ppermute | solution.py:433
  51.4 0.8 collective-permute-start.7
  52.1 2.9 %collective-permute-start.11 = (bf16[256,512]{1,0:T(8,128)(2,1)S(1)}, bf16[256,512]{1,0:T(8,128)(2,1)S(1)}, u32[]{:S(2)}, u32[]{:S(2)}) collective-permute-start(bf16[256,512]{1,0:T(8,128)(2,1)S(1)} %get-tuple-element.42), channel_id=1, source_target_pairs={{0,4},{2,6},{4,0},{6,2},{1,5},{3,7},{5,1},{7,3},{8,12},{10,14},{12... | collective-permute-start | bytes 786440 | tf_op jit(solution)/shard_map/ppermute | solution.py:433
  55.1 0.9 %collective-permute-start.12 = (bf16[256,512]{1,0:T(8,128)(2,1)S(1)}, bf16[256,512]{1,0:T(8,128)(2,1)S(1)}, u32[]{:S(2)}, u32[]{:S(2)}) collective-permute-start(bf16[256,512]{1,0:T(8,128)(2,1)S(1)} %get-tuple-element.43), channel_id=1, source_target_pairs={{0,6},{2,0},{4,2},{6,4},{1,7},{3,1},{5,3},{7,5},{8,14},{10,8},{12,... | collective-permute-start | bytes 786440 | tf_op jit(solution)/shard_map/ppermute | solution.py:433
  56.0 7.9 %collective-permute-done.11.refs_6_ = bf16[256,512]{1,0:T(8,128)(2,1)S(1)} collective-permute-done((bf16[256,512]{1,0:T(8,128)(2,1)S(1)}, bf16[256,512]{1,0:T(8,128)(2,1)S(1)}, u32[]{:S(2)}, u32[]{:S(2)}) %collective-permute-start.11) | collective-permute-done | bytes 262176 | tf_op jit(solution)/shard_map/ppermute | solution.py:433
  63.8 4.1 %collective-permute-done.12.refs_7_ = bf16[256,512]{1,0:T(8,128)(2,1)S(1)} collective-permute-done((bf16[256,512]{1,0:T(8,128)(2,1)S(1)}, bf16[256,512]{1,0:T(8,128)(2,1)S(1)}, u32[]{:S(2)}, u32[]{:S(2)}) %collective-permute-start.12) | collective-permute-done | bytes 262176 | tf_op jit(solution)/shard_map/ppermute | solution.py:433
  67.9 0.7 half.1.refs_8_
  69.1 8.0 %collective-permute-start.16 = (bf16[1024,256]{1,0:T(8,128)(2,1)S(1)}, bf16[1024,256]{1,0:T(8,128)(2,1)S(1)}, u32[]{:S(2)}, u32[]{:S(2)}) collective-permute-start(bf16[1024,256]{1,0:T(8,128)(2,1)S(1)} %sent.1), channel_id=1, source_target_pairs={{0,1},{1,0},{2,3},{3,2},{4,5},{5,4},{6,7},{7,6},{8,9},{9,8},{10,11... | collective-permute-start | bytes 1572872 | tf_op jit(solution)/shard_map/ppermute | solution.py:433
  77.6 1.1 %collective-permute-done.16 = bf16[1024,256]{1,0:T(8,128)(2,1)S(1)} collective-permute-done((bf16[1024,256]{1,0:T(8,128)(2,1)S(1)}, bf16[1024,256]{1,0:T(8,128)(2,1)S(1)}, u32[]{:S(2)}, u32[]{:S(2)}) %collective-permute-start.16) | collective-permute-done | bytes 524320 | tf_op jit(solution)/shard_map/ppermute | solution.py:433
  78.7 0.9 %add_convert_fusion = bf16[1024,256]{1,0:T(8,128)(2,1)} fusion(f32[1024,256]{1,0:T(8,128)S(1)} %kept.1, bf16[1024,256]{1,0:T(8,128)(2,1)S(1)} %collective-permute-done.16), kind=kLoop, calls=%fused_computation | loop fusion | flops 786432 | bytes 2097152 | tf_op jit(solution)/shard_map/convert_element_type | solution.py:492
  (26 shorter events, 3.8 us)
Async XLA Ops:
  0.0 6.2 %copy-start = (bf16[3,128]{1,0:T(4,128)(2,1)S(1)}, bf16[3,128]{1,0:T(4,128)(2,1)}, u32[]{:S(2)}) copy-start(bf16[3,128]{1,0:T(4,128)(2,1)} %taps.1) | copy-start | bytes 2308
  0.0 6.3 %copy-start.1 = (f32[128]{0:T(128)S(1)}, f32[128]{0:T(128)}, u32[]{:S(2)}) copy-start(f32[128]{0:T(128)} %param.29) | copy-start | bytes 1540
  0.0 6.3 %copy-start.2 = (f32[128]{0:T(128)S(1)}, f32[128]{0:T(128)}, u32[]{:S(2)}) copy-start(f32[128]{0:T(128)} %param.27) | copy-start | bytes 1540
  10.0 40.9 %collective-permute-start.15 = (bf16[1024,128]{1,0:T(8,128)(2,1)S(1)}, bf16[1024,128]{1,0:T(8,128)(2,1)S(1)}, u32[]{:S(2)}, u32[]{:S(2)}) collective-permute-start(bf16[1024,128]{1,0:T(8,128)(2,1)S(1)} %get-tuple-element.44.refs_0_), channel_id=1, source_target_pairs={{0,6},{2,0},{4,2},{6,4},{1,7},{3,1},{5,3},{7,5},{8,14},{10,8},{12,... | collective-permute-start | bytes 786440 | tf_op jit(solution)/shard_map/ppermute | solution.py:433
  13.4 38.0 %collective-permute-start.14 = (bf16[1024,128]{1,0:T(8,128)(2,1)S(1)}, bf16[1024,128]{1,0:T(8,128)(2,1)S(1)}, u32[]{:S(2)}, u32[]{:S(2)}) collective-permute-start(bf16[1024,128]{1,0:T(8,128)(2,1)S(1)} %get-tuple-element.44.refs_0_), channel_id=1, source_target_pairs={{0,4},{2,6},{4,0},{6,2},{1,5},{3,7},{5,1},{7,3},{8,12},{10,14},{12... | collective-permute-start | bytes 786440 | tf_op jit(solution)/shard_map/ppermute | solution.py:433
  13.9 4.9 %collective-permute-start.2 = (bf16[144,128]{1,0:T(8,128)(2,1)S(1)}, bf16[144,128]{1,0:T(8,128)(2,1)S(1)}, u32[]{:S(2)}, u32[]{:S(2)}) collective-permute-start(bf16[144,128]{1,0:T(8,128)(2,1)S(1)} %get-tuple-element.25.own), channel_id=1, source_target_pairs={{0,24},{8,0},{16,8},{24,16},{1,25},{9,1},{17,9},{25,17},{2,26},{10... | collective-permute-start | bytes 110600 | tf_op jit(solution)/shard_map/ppermute | solution.py:433
  16.6 35.5 %collective-permute-start.13 = (bf16[1024,128]{1,0:T(8,128)(2,1)S(1)}, bf16[1024,128]{1,0:T(8,128)(2,1)S(1)}, u32[]{:S(2)}, u32[]{:S(2)}) collective-permute-start(bf16[1024,128]{1,0:T(8,128)(2,1)S(1)} %get-tuple-element.44.refs_0_), channel_id=1, source_target_pairs={{0,2},{2,4},{4,6},{6,0},{1,3},{3,5},{5,7},{7,1},{8,10},{10,12},{12... | collective-permute-start | bytes 786440 | tf_op jit(solution)/shard_map/ppermute | solution.py:433
  17.2 37.8 %collective-permute-start.10 = (bf16[256,512]{1,0:T(8,128)(2,1)S(1)}, bf16[256,512]{1,0:T(8,128)(2,1)S(1)}, u32[]{:S(2)}, u32[]{:S(2)}) collective-permute-start(bf16[256,512]{1,0:T(8,128)(2,1)S(1)} %get-tuple-element.41), channel_id=1, source_target_pairs={{0,2},{2,4},{4,6},{6,0},{1,3},{3,5},{5,7},{7,1},{8,10},{10,12},{12... | collective-permute-start | bytes 786440 | tf_op jit(solution)/shard_map/ppermute | solution.py:433
  18.8 4.6 %collective-permute-start.1 = (bf16[144,128]{1,0:T(8,128)(2,1)S(1)}, bf16[144,128]{1,0:T(8,128)(2,1)S(1)}, u32[]{:S(2)}, u32[]{:S(2)}) collective-permute-start(bf16[144,128]{1,0:T(8,128)(2,1)S(1)} %get-tuple-element.25.own), channel_id=1, source_target_pairs={{0,16},{8,24},{16,0},{24,8},{1,17},{9,25},{17,1},{25,9},{2,18},{10... | collective-permute-start | bytes 110600 | tf_op jit(solution)/shard_map/ppermute | solution.py:433
  23.4 4.3 %collective-permute-start = (bf16[144,128]{1,0:T(8,128)(2,1)S(1)}, bf16[144,128]{1,0:T(8,128)(2,1)S(1)}, u32[]{:S(2)}, u32[]{:S(2)}) collective-permute-start(bf16[144,128]{1,0:T(8,128)(2,1)S(1)} %get-tuple-element.25.own), channel_id=1, source_target_pairs={{0,8},{8,16},{16,24},{24,0},{1,9},{9,17},{17,25},{25,1},{2,10},{10... | collective-permute-start | bytes 110600 | tf_op jit(solution)/shard_map/ppermute | solution.py:433
  27.8 6.7 %collective-permute-start.4 = (bf16[144,128]{1,0:T(8,128)(2,1)S(1)}, bf16[144,128]{1,0:T(8,128)(2,1)S(1)}, u32[]{:S(2)}, u32[]{:S(2)}) collective-permute-start(bf16[144,128]{1,0:T(8,128)(2,1)S(1)} %get-tuple-element.26.own.row_total), channel_id=1, source_target_pairs={{0,224},{32,0},{64,32},{96,64},{128,96},{160,128},{192,160},{224,1... | collective-permute-start | bytes 110600 | tf_op jit(solution)/shard_map/ppermute | solution.py:433
  34.5 4.6 %collective-permute-start.3 = (bf16[144,128]{1,0:T(8,128)(2,1)S(1)}, bf16[144,128]{1,0:T(8,128)(2,1)S(1)}, u32[]{:S(2)}, u32[]{:S(2)}) collective-permute-start(bf16[144,128]{1,0:T(8,128)(2,1)S(1)} %get-tuple-element.26.own.row_total), channel_id=1, source_target_pairs={{0,32},{32,64},{64,96},{96,128},{128,160},{160,192},{192,224},{224... | collective-permute-start | bytes 110600 | tf_op jit(solution)/shard_map/ppermute | solution.py:433
  39.1 6.7 %collective-permute-start.6 = (bf16[144,128]{1,0:T(8,128)(2,1)S(1)}, bf16[144,128]{1,0:T(8,128)(2,1)S(1)}, u32[]{:S(2)}, u32[]{:S(2)}) collective-permute-start(bf16[144,128]{1,0:T(8,128)(2,1)S(1)} %column.1), channel_id=1, source_target_pairs={{0,96},{32,128},{64,160},{96,192},{128,224},{160,0},{192,32},{224,... | collective-permute-start | bytes 110600 | tf_op jit(solution)/shard_map/ppermute | solution.py:433
  45.8 3.7 %collective-permute-start.5 = (bf16[144,128]{1,0:T(8,128)(2,1)S(1)}, bf16[144,128]{1,0:T(8,128)(2,1)S(1)}, u32[]{:S(2)}, u32[]{:S(2)}) collective-permute-start(bf16[144,128]{1,0:T(8,128)(2,1)S(1)} %column.1), channel_id=1, source_target_pairs={{0,192},{32,224},{64,0},{96,32},{128,64},{160,96},{192,128},{224,1... | collective-permute-start | bytes 110600 | tf_op jit(solution)/shard_map/ppermute | solution.py:433
  49.9 18.7 %collective-permute-start.9 = (bf16[1040,128]{1,0:T(8,128)(2,1)S(1)}, bf16[1040,128]{1,0:T(8,128)(2,1)S(1)}, u32[]{:S(2)}, u32[]{:S(2)}) collective-permute-start(bf16[1040,128]{1,0:T(8,128)(2,1)S(1)} %finish.1.refs_0_), channel_id=1, source_target_pairs={{0,6},{2,0},{4,2},{6,4},{1,7},{3,1},{5,3},{7,5},{8,14},{10,8},{12,... | collective-permute-start | bytes 798728 | tf_op jit(solution)/shard_map/ppermute | solution.py:433
  50.9 17.7 %collective-permute-start.8 = (bf16[1040,128]{1,0:T(8,128)(2,1)S(1)}, bf16[1040,128]{1,0:T(8,128)(2,1)S(1)}, u32[]{:S(2)}, u32[]{:S(2)}) collective-permute-start(bf16[1040,128]{1,0:T(8,128)(2,1)S(1)} %finish.1.refs_0_), channel_id=1, source_target_pairs={{0,4},{2,6},{4,0},{6,2},{1,5},{3,7},{5,1},{7,3},{8,12},{10,14},{12... | collective-permute-start | bytes 798728 | tf_op jit(solution)/shard_map/ppermute | solution.py:433
  51.4 17.3 %collective-permute-start.7 = (bf16[1040,128]{1,0:T(8,128)(2,1)S(1)}, bf16[1040,128]{1,0:T(8,128)(2,1)S(1)}, u32[]{:S(2)}, u32[]{:S(2)}) collective-permute-start(bf16[1040,128]{1,0:T(8,128)(2,1)S(1)} %finish.1.refs_0_), channel_id=1, source_target_pairs={{0,2},{2,4},{4,6},{6,0},{1,3},{3,5},{5,7},{7,1},{8,10},{10,12},{12... | collective-permute-start | bytes 798728 | tf_op jit(solution)/shard_map/ppermute | solution.py:433
  52.1 11.7 %collective-permute-start.11 = (bf16[256,512]{1,0:T(8,128)(2,1)S(1)}, bf16[256,512]{1,0:T(8,128)(2,1)S(1)}, u32[]{:S(2)}, u32[]{:S(2)}) collective-permute-start(bf16[256,512]{1,0:T(8,128)(2,1)S(1)} %get-tuple-element.42), channel_id=1, source_target_pairs={{0,4},{2,6},{4,0},{6,2},{1,5},{3,7},{5,1},{7,3},{8,12},{10,14},{12... | collective-permute-start | bytes 786440 | tf_op jit(solution)/shard_map/ppermute | solution.py:433
  55.1 12.9 %collective-permute-start.12 = (bf16[256,512]{1,0:T(8,128)(2,1)S(1)}, bf16[256,512]{1,0:T(8,128)(2,1)S(1)}, u32[]{:S(2)}, u32[]{:S(2)}) collective-permute-start(bf16[256,512]{1,0:T(8,128)(2,1)S(1)} %get-tuple-element.43), channel_id=1, source_target_pairs={{0,6},{2,0},{4,2},{6,4},{1,7},{3,1},{5,3},{7,5},{8,14},{10,8},{12,... | collective-permute-start | bytes 786440 | tf_op jit(solution)/shard_map/ppermute | solution.py:433
  69.1 9.5 %collective-permute-start.16 = (bf16[1024,256]{1,0:T(8,128)(2,1)S(1)}, bf16[1024,256]{1,0:T(8,128)(2,1)S(1)}, u32[]{:S(2)}, u32[]{:S(2)}) collective-permute-start(bf16[1024,256]{1,0:T(8,128)(2,1)S(1)} %sent.1), channel_id=1, source_target_pairs={{0,1},{1,0},{2,3},{3,2},{4,5},{5,4},{6,7},{7,6},{8,9},{9,8},{10,11... | collective-permute-start | bytes 1572872 | tf_op jit(solution)/shard_map/ppermute | solution.py:433

commit v3 on v2

--- a/solution.py
+++ b/solution.py
@@ -32,6 +32,10 @@
     return x * jax.nn.sigmoid(x)
 
 
+def beside(ref, first, last):
+    return jnp.concatenate([ref[j] for j in range(first, last)], axis=1)
+
+
 def put_message(ref, state, decay, rim):
     high = decay.astype(bf16)
     low = (decay - high.astype(f32)).astype(bf16)
@@ -71,14 +75,16 @@
     got_gain = bring(gain_h, gain)
     half = FRONT // 2
     got_first = [bring(tokens_h.at[pl.ds(at, half)], tokens.at[pl.ds(at, half)]) for at in (0, half)]
-    got_weights = [bring(w, weights.at[:, pl.ds(j * F, F)]) for j, w in enumerate((wf_h, wi_h))]
-    others = [bring(floor_h, floor), bring(leak_h, leak)]
-    others += [
-        bring(tokens_h.at[pl.ds(at, FRONT)], tokens.at[pl.ds(at, FRONT)]) for at in range(FRONT, count, FRONT)
+    got_weights = [bring(w, weights.at[j]) for j, w in enumerate((wf_h, wi_h))]
+    others = [bring(floor_h, floor)]
+    got_tokens = [bring(tokens_h.at[pl.ds(FRONT, FRONT)], tokens.at[pl.ds(FRONT, FRONT)])]
+    others.append(bring(leak_h, leak))
+    got_tokens += [
+        bring(tokens_h.at[pl.ds(at, FRONT)], tokens.at[pl.ds(at, FRONT)]) for at in range(2 * FRONT, count, FRONT)
     ]
-    last_copies = [bring(wh_h, later.at[:, pl.ds(0, F)]), bring(wc_h, later.at[:, pl.ds(F, F)])]
+    last_copies = [bring(wh_h, later.at[0]), bring(wc_h, later.at[1])]
     last_copies += [bring(ostate_h, ostate), bring(oconv_h, oconv)]
-    next_copies = [bring(w, later.at[:, pl.ds((2 + j) * F, F)]) for j, w in enumerate((wb_h, wq_h, wg_h))]
+    next_copies = [bring(w, later.at[2 + j]) for j, w in enumerate((wb_h, wq_h, wg_h))]
 
     row = lax.broadcasted_iota(jnp.int32, (STEP, STEP), 0)
     col = lax.broadcasted_iota(jnp.int32, (STEP, STEP), 1)
@@ -94,7 +100,7 @@
 
     def project(top):
         scale = scales[top : top + FRONT]
-        found = dot(tokens[top : top + FRONT], weights[...])
+        found = dot(tokens[top : top + FRONT], beside(weights, 0, 2))
         return (found * jnp.concatenate([scale, scale], axis=1)).astype(bf16)
 
     def gates(top, found, state, total):
@@ -125,9 +131,13 @@
     for copy in got_weights:
         copy.wait()
     found = project(0)
-    for copy in others:
-        copy.wait()
     for top in range(FRONT, count, FRONT):
+        if top == FRONT:
+            for copy in others + got_tokens[:1]:
+                copy.wait()
+        if top == 2 * FRONT:
+            for copy in got_tokens[1:]:
+                copy.wait()
         norm(top, FRONT)
         following = project(top)
         state, total = gates(top - FRONT, found, state, total)
@@ -135,7 +145,7 @@
     for copy in last_copies:
         copy.wait()
     scale = scales[count - 16 :]
-    edge = dot(tokens[count - 16 :], later[:, : 2 * F]) * jnp.concatenate([scale, scale], axis=1)
+    edge = dot(tokens[count - 16 :], beside(later, 0, 2)) * jnp.concatenate([scale, scale], axis=1)
     edge = edge.astype(bf16).astype(f32)
     state, total = gates(count - FRONT, found, state, total)
     put_message(message, state, jnp.exp(total), (edge[:, :F] * edge[:, F:])[14:])
@@ -175,12 +185,12 @@
             jax.ShapeDtypeStruct((count, F), f32),
             jax.ShapeDtypeStruct((count, F), bf16),
             jax.ShapeDtypeStruct((count, F), f32),
-            jax.ShapeDtypeStruct((width, 5 * F), bf16),
+            jax.ShapeDtypeStruct((5, width, F), bf16),
         ]
         + [jax.ShapeDtypeStruct((2 * F, 4 * F), bf16)] * 4,
         scratch_shapes=[
             pltpu.VMEM((1, width), f32),
-            pltpu.VMEM((width, 2 * F), bf16),
+            pltpu.VMEM((2, width, F), bf16),
             pltpu.VMEM((1, F), f32),
             pltpu.VMEM((count, F), f32),
             pltpu.VMEM(ostate.shape, bf16),
@@ -197,7 +207,7 @@
     window[:8] = jnp.zeros((8, F), f32)
 
     def project(top, first, last):
-        found = dot(normed[top : top + FRONT], weights[:, first * F : last * F])
+        found = dot(normed[top : top + FRONT], beside(weights, first, last))
         return (found * jnp.concatenate([scales[top : top + FRONT]] * (last - first), axis=1)).astype(bf16)
 
     def convolve(top, found):
@@ -286,7 +296,7 @@
 def row_kernel(place_ref, own, one, two, three, total, before, fade):
     _, y, _, _ = unpack_place(place_ref)
     parts = [get_message(r) for r in (own, one, two, three)]
-    place = [jnp.where(y >= d, y - d, y - d + 4) for d in range(4)]
+    place = [y ^ d for d in range(4)]
     whole, inside = 0.0, 0.0
     product, product_before = 1.0, 1.0
     for d, (state, decay) in enumerate(parts):
@@ -302,7 +312,8 @@
         inside = inside + state * jnp.where(place[d] < y, between, 0.0)
         product = product * decay
         product_before = product_before * jnp.where(place[d] < y, decay, 1.0)
-    put_message(total, whole, product, get_rim(one))
+    rim = jnp.where((y & 1) > 0, get_rim(one), get_rim(three))
+    put_message(total, whole, product, rim)
     before[...] = inside
     fade[...] = jnp.broadcast_to(product_before, fade.shape)
 
@@ -431,6 +442,11 @@
 def turned(array, axis, by):
     count = lax.axis_size(axis)
     return lax.ppermute(array, axis, [(i, (i + by) % count) for i in range(count)])
+
+
+def swapped(array, axis, bits):
+    count = lax.axis_size(axis)
+    return lax.ppermute(array, axis, [(i, i ^ bits) for i in range(count)])
 
 
 def body(
@@ -470,7 +486,7 @@
         out_state,
         out_conv,
     )
-    near = [turned(message, "y", d) for d in (1, 2, 3)]
+    near = [swapped(message, "y", d) for d in (1, 2, 3)]
     columns = columns[:1] + [turned(columns[d], "x", d) for d in (1, 2, 3)]
     heads, extra, conv_res = conv(
         normed, scales, later, conv_taps, line(group_gain), line(state_gain)

time: 79.7 us -> 77.8 us (0.976)
  waiting for transfers between devices: 34.4 us -> 30.7 us
  starting transfers between devices: 30.4 us -> 32.5 us
    ppermute x17 -> x14, waiting for transfers between devices: 34.4 us -> 24.1 us  [turned(): lax.ppermute(array, axis, [(i, (i + by) % count) for i in range(count)])]
    ppermute x0 -> x3, waiting for transfers between devices: none -> 6.56 us  [swapped(): return lax.ppermute(array, axis, [(i, i ^ bits) for i in range(count)])]
    ppermute x0 -> x3, starting transfers between devices: none -> 3.9 us  [swapped(): return lax.ppermute(array, axis, [(i, i ^ bits) for i in range(count)])]
    ppermute x17 -> x14, starting transfers between devices: 30.4 us -> 28.6 us  [turned(): lax.ppermute(array, axis, [(i, (i + by) % count) for i in range(count)])]
where the time goes in v3:
time: 77.8 us; the launch traced here: 77.7 us
  starting transfers between devices  32.5 us (42%)
  waiting for transfers between devices  30.7 us (39%)
  Pallas kernels  13.4 us (17%)
  other arithmetic  0.95 us (1%)
    ppermute x14, starting transfers between devices, turned(): lax.ppermute(array, axis, [(i, (i + by) % count) for i in range(count)])  28.6 us
    ppermute x14, waiting for transfers between devices, turned(): lax.ppermute(array, axis, [(i, (i + by) % count) for i in range(count)])  24.1 us
    ppermute x3, waiting for transfers between devices, swapped(): return lax.ppermute(array, axis, [(i, i ^ bits) for i in range(count)])  6.56 us
    pallas_call x1, Pallas kernels, front(): pl.pallas_call(front_kernel, in_specs=[pl.BlockSpec(memory_space=pltpu.SM...  5.93 us
    ppermute x3, starting transfers between devices, swapped(): return lax.ppermute(array, axis, [(i, i ^ bits) for i in range(count)])  3.9 us
    pallas_call x1, Pallas kernels, conv(): pl.pallas_call(conv_kernel, in_specs=[vmem] * 6, out_specs=[vmem] * 3, ou...  3.68 us
    pallas_call x1, Pallas kernels, read(): pl.pallas_call(read_kernel, in_specs=[vmem] * 5, out_specs=[vmem] * 3, ou...  1.65 us
  transfers between devices with their start and end apart: 17, of which 9 were waited for; matrix products, arithmetic and copies ran while one was open for 0% of the time, Pallas kernels for 4%

profile of v3, /device:TPU:1, one launch (start us, length us, event | category | flops | bytes accessed | tf_op | source)
XLA Modules:
  0.0 77.7 jit_solution(2220292422658807310)
XLA Ops:
  0.0 5.9 %front.1 = (bf16[1024,2048]{1,0:T(8,128)(2,1)S(1)}, f32[1024,128]{1,0:T(8,128)S(1)}, bf16[144,128]{1,0:T(8,128)(2,1)S(1)}, f32[1024,128]{1,0:T(8,128)S(1)}, bf16...) custom-call(s32[1]{0:T(128)} %bitcast.place.place_ref, ...), custom_call_target="tpu_custom_call" | custom-call | tf_op jit(solution)/shard_map/front/pallas_call | solution.py:177
  6.0 3.7 %conv.1 = (bf16[1024,256]{1,0:T(8,128)(2,1)S(1)}, f32[40,128]{1,0:T(8,128)S(1)}, bf16[1024,128]{1,0:T(8,128)(2,1)S(1)}) custom-call(bf16[1024,2048]{1,0:T(8,128)(2,1)S(1)} %get-tuple-element.29.normed, f32[1024,128]{1,0:T(8,128)S(1)} %get-tuple-element.30.scales, bf16[5,2048,128]{2,1,0:T(8,128)(2,1)S(1)} %get-tuple-element.31.weights, ...), custom_call_target="tpu_custom_call" | custom-call | tf_op jit(solution)/shard_map/conv/pallas_call | solution.py:238
  9.7 3.4 %collective-permute-start.15 = (bf16[1024,128]{1,0:T(8,128)(2,1)S(1)}, bf16[1024,128]{1,0:T(8,128)(2,1)S(1)}, u32[]{:S(2)}, u32[]{:S(2)}) collective-permute-start(bf16[1024,128]{1,0:T(8,128)(2,1)S(1)} %get-tuple-element.44.refs_0_), channel_id=1, source_target_pairs={{0,6},{2,0},{4,2},{6,4},{1,7},{3,1},{5,3},{7,5},{8,14},{10,8},{12,... | collective-permute-start | bytes 786440 | tf_op jit(solution)/shard_map/ppermute | solution.py:444
  13.6 2.7 %collective-permute-start.2 = (bf16[144,128]{1,0:T(8,128)(2,1)S(1)}, bf16[144,128]{1,0:T(8,128)(2,1)S(1)}, u32[]{:S(2)}, u32[]{:S(2)}) collective-permute-start(bf16[144,128]{1,0:T(8,128)(2,1)S(1)} %get-tuple-element.25.own), channel_id=1, source_target_pairs={{0,24},{8,16},{16,8},{24,0},{1,25},{9,17},{17,9},{25,1},{2,26},{10... | collective-permute-start | bytes 110600 | tf_op jit(solution)/shard_map/ppermute | solution.py:449
  16.9 1.5 %collective-permute-start.10 = (bf16[256,512]{1,0:T(8,128)(2,1)S(1)}, bf16[256,512]{1,0:T(8,128)(2,1)S(1)}, u32[]{:S(2)}, u32[]{:S(2)}) collective-permute-start(bf16[256,512]{1,0:T(8,128)(2,1)S(1)} %get-tuple-element.41), channel_id=1, source_target_pairs={{0,2},{2,4},{4,6},{6,0},{1,3},{3,5},{5,7},{7,1},{8,10},{10,12},{12... | collective-permute-start | bytes 786440 | tf_op jit(solution)/shard_map/ppermute | solution.py:444
  18.4 1.2 %collective-permute-start.1 = (bf16[144,128]{1,0:T(8,128)(2,1)S(1)}, bf16[144,128]{1,0:T(8,128)(2,1)S(1)}, u32[]{:S(2)}, u32[]{:S(2)}) collective-permute-start(bf16[144,128]{1,0:T(8,128)(2,1)S(1)} %get-tuple-element.25.own), channel_id=1, source_target_pairs={{0,16},{8,24},{16,0},{24,8},{1,17},{9,25},{17,1},{25,9},{2,18},{10... | collective-permute-start | bytes 110600 | tf_op jit(solution)/shard_map/ppermute | solution.py:449
  19.6 3.5 %collective-permute-done.1.two = bf16[144,128]{1,0:T(8,128)(2,1)S(1)} collective-permute-done((bf16[144,128]{1,0:T(8,128)(2,1)S(1)}, bf16[144,128]{1,0:T(8,128)(2,1)S(1)}, u32[]{:S(2)}, u32[]{:S(2)}) %collective-permute-start.1) | collective-permute-done | bytes 36896 | tf_op jit(solution)/shard_map/ppermute | solution.py:449
  23.0 3.1 %collective-permute-done.one = bf16[144,128]{1,0:T(8,128)(2,1)S(1)} collective-permute-done((bf16[144,128]{1,0:T(8,128)(2,1)S(1)}, bf16[144,128]{1,0:T(8,128)(2,1)S(1)}, u32[]{:S(2)}, u32[]{:S(2)}) %collective-permute-start) | collective-permute-done | bytes 36896 | tf_op jit(solution)/shard_map/ppermute | solution.py:449
  26.2 5.8 %collective-permute-start.4 = (bf16[144,128]{1,0:T(8,128)(2,1)S(1)}, bf16[144,128]{1,0:T(8,128)(2,1)S(1)}, u32[]{:S(2)}, u32[]{:S(2)}) collective-permute-start(bf16[144,128]{1,0:T(8,128)(2,1)S(1)} %get-tuple-element.26.own.row_total), channel_id=1, source_target_pairs={{0,224},{32,0},{64,32},{96,64},{128,96},{160,128},{192,160},{224,1... | collective-permute-start | bytes 110600 | tf_op jit(solution)/shard_map/ppermute | solution.py:444
  32.0 1.1 %collective-permute-done.4.ahead = bf16[144,128]{1,0:T(8,128)(2,1)S(1)} collective-permute-done((bf16[144,128]{1,0:T(8,128)(2,1)S(1)}, bf16[144,128]{1,0:T(8,128)(2,1)S(1)}, u32[]{:S(2)}, u32[]{:S(2)}) %collective-permute-start.4) | collective-permute-done | bytes 36896 | tf_op jit(solution)/shard_map/ppermute | solution.py:444
  33.1 4.6 %collective-permute-done.3.behind.near = bf16[144,128]{1,0:T(8,128)(2,1)S(1)} collective-permute-done((bf16[144,128]{1,0:T(8,128)(2,1)S(1)}, bf16[144,128]{1,0:T(8,128)(2,1)S(1)}, u32[]{:S(2)}, u32[]{:S(2)}) %collective-permute-start.3) | collective-permute-done | bytes 36896 | tf_op jit(solution)/shard_map/ppermute | solution.py:444
  38.5 5.3 %collective-permute-done.6.three = bf16[144,128]{1,0:T(8,128)(2,1)S(1)} collective-permute-done((bf16[144,128]{1,0:T(8,128)(2,1)S(1)}, bf16[144,128]{1,0:T(8,128)(2,1)S(1)}, u32[]{:S(2)}, u32[]{:S(2)}) %collective-permute-start.6) | collective-permute-done | bytes 36896 | tf_op jit(solution)/shard_map/ppermute | solution.py:444
  43.8 0.9 %collective-permute-start.5 = (bf16[144,128]{1,0:T(8,128)(2,1)S(1)}, bf16[144,128]{1,0:T(8,128)(2,1)S(1)}, u32[]{:S(2)}, u32[]{:S(2)}) collective-permute-start(bf16[144,128]{1,0:T(8,128)(2,1)S(1)} %column.1), channel_id=1, source_target_pairs={{0,192},{32,224},{64,0},{96,32},{128,64},{160,96},{192,128},{224,1... | collective-permute-start | bytes 110600 | tf_op jit(solution)/shard_map/ppermute | solution.py:444
  44.7 1.7 %read.1 = (f32[1024,128]{1,0:T(8,128)S(1)}, bf16[1024,128]{1,0:T(8,128)(2,1)S(1)}, f32[1024,128]{1,0:T(8,128)S(1)}) custom-call(bf16[1024,256]{1,0:T(8,128)(2,1)S(1)} %get-tuple-element.32.heads, f32[40,128]{1,0:T(8,128)S(1)} %get-tuple-element.33.extra, f32[1024,128]{1,0:T(8,128)S(1)} %get-tuple-element.34.keys, ...), custom_call_target="tpu_custom_call" | custom-call | tf_op jit(solution)/shard_map/read/pallas_call | solution.py:282
  46.4 1.2 %collective-permute-done.5.six = bf16[144,128]{1,0:T(8,128)(2,1)S(1)} collective-permute-done((bf16[144,128]{1,0:T(8,128)(2,1)S(1)}, bf16[144,128]{1,0:T(8,128)(2,1)S(1)}, u32[]{:S(2)}, u32[]{:S(2)}) %collective-permute-start.5) | collective-permute-done | bytes 36896 | tf_op jit(solution)/shard_map/ppermute | solution.py:444
  48.0 1.5 %collective-permute-start.9 = (bf16[1040,128]{1,0:T(8,128)(2,1)S(1)}, bf16[1040,128]{1,0:T(8,128)(2,1)S(1)}, u32[]{:S(2)}, u32[]{:S(2)}) collective-permute-start(bf16[1040,128]{1,0:T(8,128)(2,1)S(1)} %finish.1.refs_0_), channel_id=1, source_target_pairs={{0,6},{2,0},{4,2},{6,4},{1,7},{3,1},{5,3},{7,5},{8,14},{10,8},{12,... | collective-permute-start | bytes 798728 | tf_op jit(solution)/shard_map/ppermute | solution.py:444
  49.5 1.0 %collective-permute-start.8 = (bf16[1040,128]{1,0:T(8,128)(2,1)S(1)}, bf16[1040,128]{1,0:T(8,128)(2,1)S(1)}, u32[]{:S(2)}, u32[]{:S(2)}) collective-permute-start(bf16[1040,128]{1,0:T(8,128)(2,1)S(1)} %finish.1.refs_0_), channel_id=1, source_target_pairs={{0,4},{2,6},{4,0},{6,2},{1,5},{3,7},{5,1},{7,3},{8,12},{10,14},{12... | collective-permute-start | bytes 798728 | tf_op jit(solution)/shard_map/ppermute | solution.py:444
  51.3 1.9 %collective-permute-start.11 = (bf16[256,512]{1,0:T(8,128)(2,1)S(1)}, bf16[256,512]{1,0:T(8,128)(2,1)S(1)}, u32[]{:S(2)}, u32[]{:S(2)}) collective-permute-start(bf16[256,512]{1,0:T(8,128)(2,1)S(1)} %get-tuple-element.42), channel_id=1, source_target_pairs={{0,4},{2,6},{4,0},{6,2},{1,5},{3,7},{5,1},{7,3},{8,12},{10,14},{12... | collective-permute-start | bytes 786440 | tf_op jit(solution)/shard_map/ppermute | solution.py:444
  53.2 1.4 %collective-permute-start.12 = (bf16[256,512]{1,0:T(8,128)(2,1)S(1)}, bf16[256,512]{1,0:T(8,128)(2,1)S(1)}, u32[]{:S(2)}, u32[]{:S(2)}) collective-permute-start(bf16[256,512]{1,0:T(8,128)(2,1)S(1)} %get-tuple-element.43), channel_id=1, source_target_pairs={{0,6},{2,0},{4,2},{6,4},{1,7},{3,1},{5,3},{7,5},{8,14},{10,8},{12,... | collective-permute-start | bytes 786440 | tf_op jit(solution)/shard_map/ppermute | solution.py:444
  54.6 8.2 %collective-permute-done.11.refs_6_ = bf16[256,512]{1,0:T(8,128)(2,1)S(1)} collective-permute-done((bf16[256,512]{1,0:T(8,128)(2,1)S(1)}, bf16[256,512]{1,0:T(8,128)(2,1)S(1)}, u32[]{:S(2)}, u32[]{:S(2)}) %collective-permute-start.11) | collective-permute-done | bytes 262176 | tf_op jit(solution)/shard_map/ppermute | solution.py:444
  62.8 2.7 %collective-permute-done.12.refs_7_ = bf16[256,512]{1,0:T(8,128)(2,1)S(1)} collective-permute-done((bf16[256,512]{1,0:T(8,128)(2,1)S(1)}, bf16[256,512]{1,0:T(8,128)(2,1)S(1)}, u32[]{:S(2)}, u32[]{:S(2)}) %collective-permute-start.12) | collective-permute-done | bytes 262176 | tf_op jit(solution)/shard_map/ppermute | solution.py:444
  66.7 8.5 %collective-permute-start.16 = (bf16[1024,256]{1,0:T(8,128)(2,1)S(1)}, bf16[1024,256]{1,0:T(8,128)(2,1)S(1)}, u32[]{:S(2)}, u32[]{:S(2)}) collective-permute-start(bf16[1024,256]{1,0:T(8,128)(2,1)S(1)} %sent.1), channel_id=1, source_target_pairs={{0,1},{1,0},{2,3},{3,2},{4,5},{5,4},{6,7},{7,6},{8,9},{9,8},{10,11... | collective-permute-start | bytes 1572872 | tf_op jit(solution)/shard_map/ppermute | solution.py:444
  75.7 1.1 %collective-permute-done.16 = bf16[1024,256]{1,0:T(8,128)(2,1)S(1)} collective-permute-done((bf16[1024,256]{1,0:T(8,128)(2,1)S(1)}, bf16[1024,256]{1,0:T(8,128)(2,1)S(1)}, u32[]{:S(2)}, u32[]{:S(2)}) %collective-permute-start.16) | collective-permute-done | bytes 524320 | tf_op jit(solution)/shard_map/ppermute | solution.py:444
  76.8 0.9 %add_convert_fusion = bf16[1024,256]{1,0:T(8,128)(2,1)} fusion(f32[1024,256]{1,0:T(8,128)S(1)} %kept.1, bf16[1024,256]{1,0:T(8,128)(2,1)S(1)} %collective-permute-done.16), kind=kLoop, calls=%fused_computation | loop fusion | flops 786432 | bytes 2097152 | tf_op jit(solution)/shard_map/convert_element_type | solution.py:508
  (26 shorter events, 4.8 us)
Async XLA Ops:
  0.0 6.0 %copy-start = (bf16[3,128]{1,0:T(4,128)(2,1)S(1)}, bf16[3,128]{1,0:T(4,128)(2,1)}, u32[]{:S(2)}) copy-start(bf16[3,128]{1,0:T(4,128)(2,1)} %taps.1) | copy-start | bytes 2308
  0.0 6.0 %copy-start.1 = (f32[128]{0:T(128)S(1)}, f32[128]{0:T(128)}, u32[]{:S(2)}) copy-start(f32[128]{0:T(128)} %param.29) | copy-start | bytes 1540
  0.0 6.0 %copy-start.2 = (f32[128]{0:T(128)S(1)}, f32[128]{0:T(128)}, u32[]{:S(2)}) copy-start(f32[128]{0:T(128)} %param.27) | copy-start | bytes 1540
  9.7 39.8 %collective-permute-start.15 = (bf16[1024,128]{1,0:T(8,128)(2,1)S(1)}, bf16[1024,128]{1,0:T(8,128)(2,1)S(1)}, u32[]{:S(2)}, u32[]{:S(2)}) collective-permute-start(bf16[1024,128]{1,0:T(8,128)(2,1)S(1)} %get-tuple-element.44.refs_0_), channel_id=1, source_target_pairs={{0,6},{2,0},{4,2},{6,4},{1,7},{3,1},{5,3},{7,5},{8,14},{10,8},{12,... | collective-permute-start | bytes 786440 | tf_op jit(solution)/shard_map/ppermute | solution.py:444
  13.0 37.5 %collective-permute-start.14 = (bf16[1024,128]{1,0:T(8,128)(2,1)S(1)}, bf16[1024,128]{1,0:T(8,128)(2,1)S(1)}, u32[]{:S(2)}, u32[]{:S(2)}) collective-permute-start(bf16[1024,128]{1,0:T(8,128)(2,1)S(1)} %get-tuple-element.44.refs_0_), channel_id=1, source_target_pairs={{0,4},{2,6},{4,0},{6,2},{1,5},{3,7},{5,1},{7,3},{8,12},{10,14},{12... | collective-permute-start | bytes 786440 | tf_op jit(solution)/shard_map/ppermute | solution.py:444
  13.6 4.9 %collective-permute-start.2 = (bf16[144,128]{1,0:T(8,128)(2,1)S(1)}, bf16[144,128]{1,0:T(8,128)(2,1)S(1)}, u32[]{:S(2)}, u32[]{:S(2)}) collective-permute-start(bf16[144,128]{1,0:T(8,128)(2,1)S(1)} %get-tuple-element.25.own), channel_id=1, source_target_pairs={{0,24},{8,16},{16,8},{24,0},{1,25},{9,17},{17,9},{25,1},{2,26},{10... | collective-permute-start | bytes 110600 | tf_op jit(solution)/shard_map/ppermute | solution.py:449
  16.3 35.0 %collective-permute-start.13 = (bf16[1024,128]{1,0:T(8,128)(2,1)S(1)}, bf16[1024,128]{1,0:T(8,128)(2,1)S(1)}, u32[]{:S(2)}, u32[]{:S(2)}) collective-permute-start(bf16[1024,128]{1,0:T(8,128)(2,1)S(1)} %get-tuple-element.44.refs_0_), channel_id=1, source_target_pairs={{0,2},{2,4},{4,6},{6,0},{1,3},{3,5},{5,7},{7,1},{8,10},{10,12},{12... | collective-permute-start | bytes 786440 | tf_op jit(solution)/shard_map/ppermute | solution.py:444
  16.9 36.3 %collective-permute-start.10 = (bf16[256,512]{1,0:T(8,128)(2,1)S(1)}, bf16[256,512]{1,0:T(8,128)(2,1)S(1)}, u32[]{:S(2)}, u32[]{:S(2)}) collective-permute-start(bf16[256,512]{1,0:T(8,128)(2,1)S(1)} %get-tuple-element.41), channel_id=1, source_target_pairs={{0,2},{2,4},{4,6},{6,0},{1,3},{3,5},{5,7},{7,1},{8,10},{10,12},{12... | collective-permute-start | bytes 786440 | tf_op jit(solution)/shard_map/ppermute | solution.py:444
  18.4 4.6 %collective-permute-start.1 = (bf16[144,128]{1,0:T(8,128)(2,1)S(1)}, bf16[144,128]{1,0:T(8,128)(2,1)S(1)}, u32[]{:S(2)}, u32[]{:S(2)}) collective-permute-start(bf16[144,128]{1,0:T(8,128)(2,1)S(1)} %get-tuple-element.25.own), channel_id=1, source_target_pairs={{0,16},{8,24},{16,0},{24,8},{1,17},{9,25},{17,1},{25,9},{2,18},{10... | collective-permute-start | bytes 110600 | tf_op jit(solution)/shard_map/ppermute | solution.py:449
  23.0 3.1 %collective-permute-start = (bf16[144,128]{1,0:T(8,128)(2,1)S(1)}, bf16[144,128]{1,0:T(8,128)(2,1)S(1)}, u32[]{:S(2)}, u32[]{:S(2)}) collective-permute-start(bf16[144,128]{1,0:T(8,128)(2,1)S(1)} %get-tuple-element.25.own), channel_id=1, source_target_pairs={{0,8},{8,0},{16,24},{24,16},{1,9},{9,1},{17,25},{25,17},{2,10},{10... | collective-permute-start | bytes 110600 | tf_op jit(solution)/shard_map/ppermute | solution.py:449
  26.2 6.9 %collective-permute-start.4 = (bf16[144,128]{1,0:T(8,128)(2,1)S(1)}, bf16[144,128]{1,0:T(8,128)(2,1)S(1)}, u32[]{:S(2)}, u32[]{:S(2)}) collective-permute-start(bf16[144,128]{1,0:T(8,128)(2,1)S(1)} %get-tuple-element.26.own.row_total), channel_id=1, source_target_pairs={{0,224},{32,0},{64,32},{96,64},{128,96},{160,128},{192,160},{224,1... | collective-permute-start | bytes 110600 | tf_op jit(solution)/shard_map/ppermute | solution.py:444
  33.1 4.6 %collective-permute-start.3 = (bf16[144,128]{1,0:T(8,128)(2,1)S(1)}, bf16[144,128]{1,0:T(8,128)(2,1)S(1)}, u32[]{:S(2)}, u32[]{:S(2)}) collective-permute-start(bf16[144,128]{1,0:T(8,128)(2,1)S(1)} %get-tuple-element.26.own.row_total), channel_id=1, source_target_pairs={{0,32},{32,64},{64,96},{96,128},{128,160},{160,192},{192,224},{224... | collective-permute-start | bytes 110600 | tf_op jit(solution)/shard_map/ppermute | solution.py:444
  37.7 6.0 %collective-permute-start.6 = (bf16[144,128]{1,0:T(8,128)(2,1)S(1)}, bf16[144,128]{1,0:T(8,128)(2,1)S(1)}, u32[]{:S(2)}, u32[]{:S(2)}) collective-permute-start(bf16[144,128]{1,0:T(8,128)(2,1)S(1)} %column.1), channel_id=1, source_target_pairs={{0,96},{32,128},{64,160},{96,192},{128,224},{160,0},{192,32},{224,... | collective-permute-start | bytes 110600 | tf_op jit(solution)/shard_map/ppermute | solution.py:444
  43.8 3.8 %collective-permute-start.5 = (bf16[144,128]{1,0:T(8,128)(2,1)S(1)}, bf16[144,128]{1,0:T(8,128)(2,1)S(1)}, u32[]{:S(2)}, u32[]{:S(2)}) collective-permute-start(bf16[144,128]{1,0:T(8,128)(2,1)S(1)} %column.1), channel_id=1, source_target_pairs={{0,192},{32,224},{64,0},{96,32},{128,64},{160,96},{192,128},{224,1... | collective-permute-start | bytes 110600 | tf_op jit(solution)/shard_map/ppermute | solution.py:444
  48.0 18.2 %collective-permute-start.9 = (bf16[1040,128]{1,0:T(8,128)(2,1)S(1)}, bf16[1040,128]{1,0:T(8,128)(2,1)S(1)}, u32[]{:S(2)}, u32[]{:S(2)}) collective-permute-start(bf16[1040,128]{1,0:T(8,128)(2,1)S(1)} %finish.1.refs_0_), channel_id=1, source_target_pairs={{0,6},{2,0},{4,2},{6,4},{1,7},{3,1},{5,3},{7,5},{8,14},{10,8},{12,... | collective-permute-start | bytes 798728 | tf_op jit(solution)/shard_map/ppermute | solution.py:444
  49.5 16.7 %collective-permute-start.8 = (bf16[1040,128]{1,0:T(8,128)(2,1)S(1)}, bf16[1040,128]{1,0:T(8,128)(2,1)S(1)}, u32[]{:S(2)}, u32[]{:S(2)}) collective-permute-start(bf16[1040,128]{1,0:T(8,128)(2,1)S(1)} %finish.1.refs_0_), channel_id=1, source_target_pairs={{0,4},{2,6},{4,0},{6,2},{1,5},{3,7},{5,1},{7,3},{8,12},{10,14},{12... | collective-permute-start | bytes 798728 | tf_op jit(solution)/shard_map/ppermute | solution.py:444
  50.5 15.7 %collective-permute-start.7 = (bf16[1040,128]{1,0:T(8,128)(2,1)S(1)}, bf16[1040,128]{1,0:T(8,128)(2,1)S(1)}, u32[]{:S(2)}, u32[]{:S(2)}) collective-permute-start(bf16[1040,128]{1,0:T(8,128)(2,1)S(1)} %finish.1.refs_0_), channel_id=1, source_target_pairs={{0,2},{2,4},{4,6},{6,0},{1,3},{3,5},{5,7},{7,1},{8,10},{10,12},{12... | collective-permute-start | bytes 798728 | tf_op jit(solution)/shard_map/ppermute | solution.py:444
  51.3 11.5 %collective-permute-start.11 = (bf16[256,512]{1,0:T(8,128)(2,1)S(1)}, bf16[256,512]{1,0:T(8,128)(2,1)S(1)}, u32[]{:S(2)}, u32[]{:S(2)}) collective-permute-start(bf16[256,512]{1,0:T(8,128)(2,1)S(1)} %get-tuple-element.42), channel_id=1, source_target_pairs={{0,4},{2,6},{4,0},{6,2},{1,5},{3,7},{5,1},{7,3},{8,12},{10,14},{12... | collective-permute-start | bytes 786440 | tf_op jit(solution)/shard_map/ppermute | solution.py:444
  53.2 12.4 %collective-permute-start.12 = (bf16[256,512]{1,0:T(8,128)(2,1)S(1)}, bf16[256,512]{1,0:T(8,128)(2,1)S(1)}, u32[]{:S(2)}, u32[]{:S(2)}) collective-permute-start(bf16[256,512]{1,0:T(8,128)(2,1)S(1)} %get-tuple-element.43), channel_id=1, source_target_pairs={{0,6},{2,0},{4,2},{6,4},{1,7},{3,1},{5,3},{7,5},{8,14},{10,8},{12,... | collective-permute-start | bytes 786440 | tf_op jit(solution)/shard_map/ppermute | solution.py:444
  66.7 10.1 %collective-permute-start.16 = (bf16[1024,256]{1,0:T(8,128)(2,1)S(1)}, bf16[1024,256]{1,0:T(8,128)(2,1)S(1)}, u32[]{:S(2)}, u32[]{:S(2)}) collective-permute-start(bf16[1024,256]{1,0:T(8,128)(2,1)S(1)} %sent.1), channel_id=1, source_target_pairs={{0,1},{1,0},{2,3},{3,2},{4,5},{5,4},{6,7},{7,6},{8,9},{9,8},{10,11... | collective-permute-start | bytes 1572872 | tf_op jit(solution)/shard_map/ppermute | solution.py:444
